TPU v7x, 32 devices: a whole 2x2x4 slice. The times are simulated.
32 devices in a mesh: rep: 2 (over x), fs: 8 (over z, y), tp: 2 (over core).
Axes of the slice: x: 2, y: 2, z: 4, core: 2. Of those that a mesh axis runs over, the one named last changes fastest.
Arguments:
- resid: bfloat16 [16384, 2048], P(('rep', 'fs'), 'tp'), may hold values from -6 to 6
- gain_mix_in: float32 [2048], replicated, may hold values from 0.1 to 1.9
- u_weight: float32 [2048, 1024], P('fs', 'tp'), may hold values from -0.125 to 0.125
- v_weight: float32 [2048, 1024], P('fs', 'tp'), may hold values from -0.125 to 0.125
- u_scale: float32 [1024], P('tp'), may hold values from 0.5 to 2
- v_scale: float32 [1024], P('tp'), may hold values from 0.3 to 3
- v_gain: float32 [1024], P('tp'), may hold values from 0.1 to 1.9
- mix_matrix: float32 [16, 128, 128], P('tp'), may hold values from -0.5 to 0.5
- mix_bias: float32 [16, 128], P('tp'), may hold values from 0.1 to 1.9
- out_weight: float32 [1024, 2048], P('tp', 'fs'), may hold values from -0.1875 to 0.1875
- out_scale: float32 [2048], P('fs'), may hold values from 0.3 to 3
- gain_mix_out: float32 [2048], replicated, may hold values from 0.1 to 1.9
- gain_ffn_in: float32 [2048], replicated, may hold values from 0.1 to 1.9
- up_weight: float32 [2048, 4096], P('fs', 'tp'), may hold values from -0.125 to 0.125
- up_scale: float32 [4096], P('tp'), may hold values from 0.5 to 2
- down_weight: float32 [4096, 2048], P('tp', 'fs'), may hold values from -0.09375 to 0.09375
- down_scale: float32 [2048], P('fs'), may hold values from 0.3 to 3
- gain_ffn_out: float32 [2048], replicated, may hold values from 0.1 to 1.9
Outputs:
- result: bfloat16 [16384, 2048], P(('rep', 'fs'), 'tp')
All inputs are finite; a program needn't handle non-finite values.
Results may differ from a plain program's by a relative error of at most 0.013.
Values may be sent and summed in bfloat16 or wider, within the bound.
A program may use at most 128 MiB of HBM per device.

v0:
```python
import functools

import jax
import jax.numpy as jnp
from jax import lax
from jax.experimental import pallas as pl
from jax.experimental.pallas import tpu as pltpu
from jax.sharding import PartitionSpec as P


def gather_kernel(by_rows, parts, n_out, n_in, *refs):
    count = len(by_rows)
    srcs, resid = refs[:count], refs[count]
    dsts, other = refs[count + 1 : 2 * count + 1], refs[2 * count + 1]
    z_send, z_recv, y_send, y_recv, x_send, x_recv, t_send, t_recv, own_sem = refs[2 * count + 2 :]
    member = lax.axis_index("fs")
    rep = lax.axis_index("rep")
    tp = lax.axis_index("tp")
    outer, inner = member // n_in, member % n_in
    peer_in = 1 - inner
    has_left, has_right = outer > 0, outer < n_out - 1
    left, right = {"fs": member - n_in}, {"fs": member + n_in}
    across, twin, mate = {"fs": outer * n_in + peer_in}, {"rep": 1 - rep}, {"tp": 1 - tp}

    def greet(device):
        pl.semaphore_signal(barrier, inc=1, device_id=device, device_id_type=pl.DeviceIdType.MESH)

    barrier = pltpu.get_barrier_semaphore()
    for step in (1, n_out - 1):
        greet({"fs": lax.rem(outer + step, n_out) * n_in + inner})
    for device in (across, twin, mate):
        greet(device)
    pl.semaphore_wait(barrier, 5)

    def slot(part, index, first=0, length=4):
        w, low, size = parts[part]
        rows, cols = srcs[w].shape
        base, size = low + first * (size // 4), length * (size // 4)
        if by_rows[w]:
            return dsts[w].at[pl.ds(pl.multiple_of(index * rows + base, 8), size), :]
        return dsts[w].at[
            pl.ds(pl.multiple_of(base, 8), size), pl.ds(pl.multiple_of(index * cols, 128), cols)
        ]

    def remote(ref, send, recv, device):
        return pltpu.make_async_remote_copy(
            src_ref=ref,
            dst_ref=ref,
            send_sem=send,
            recv_sem=recv,
            device_id=device,
            device_id_type=pl.DeviceIdType.MESH,
        )

    swap = pltpu.make_async_remote_copy(
        src_ref=resid,
        dst_ref=other,
        send_sem=t_send,
        recv_sem=t_recv,
        device_id=mate,
        device_id_type=pl.DeviceIdType.MESH,
    )
    own = []
    for w in range(count):
        rows, cols = srcs[w].shape
        if by_rows[w]:
            place = dsts[w].at[pl.ds(pl.multiple_of(member * rows, 8), rows), :]
        else:
            place = dsts[w].at[:, pl.ds(pl.multiple_of(member * cols, 128), cols)]
        own.append(pltpu.make_async_copy(srcs[w], place, own_sem.at[w]))
        own[w].start()

    def column(index, line):
        return index * n_in + line

    def z_copy(part, way, d, piece):
        ahead = 1 if way == 0 else -1
        index = column(outer - ahead * d, inner)
        ref = slot(part, index, 2 * rep, 2) if piece == 0 else slot(part, index, 3 * (1 - rep), 1)
        return remote(
            ref,
            z_send.at[part, way, d, piece],
            z_recv.at[part, way, d, piece],
            right if way == 0 else left,
        )

    def valid(way, d):
        return outer >= d if way == 0 else outer + d <= n_out - 1

    def onward(way):
        return has_right if way == 0 else has_left

    def source_of(way, d):
        return outer - d if way == 0 else outer + d

    def y_copy(part, way, d):
        ref = slot(part, column(source_of(way, d), inner), 2 * rep, 2)
        return remote(ref, y_send.at[part, way, d], y_recv.at[part, way, d], across)

    def y_own(part):
        ref = slot(part, member)
        return remote(ref, y_send.at[part, 0, 0], y_recv.at[part, 0, 0], across)

    def x_copy(part, way, d, piece):
        if piece == 0:
            ref = slot(part, column(source_of(way, d), inner), 1 + rep, 1)
        else:
            ref = slot(part, column(source_of(way, d), peer_in), 2 * rep, 2)
        return remote(ref, x_send.at[part, way, d, piece], x_recv.at[part, way, d, piece], twin)

    def landed(part, way, d, piece):
        index = column(source_of(way, d), inner)
        ref = slot(part, index, 2 * rep, 2) if piece == 0 else slot(part, index, 3 * (1 - rep), 1)
        remote(
            ref,
            z_send.at[part, way, d - 1, piece],
            z_recv.at[part, way, d - 1, piece],
            left if way == 0 else right,
        ).wait_recv()

    for w in range(count):
        own[w].wait()
        for part, (held, _, _) in enumerate(parts):
            if held == w:
                for way in range(2):

                    @pl.when(onward(way))
                    def _():
                        z_copy(part, way, 0, 0).start()
                        z_copy(part, way, 0, 1).start()

                y_own(part).start()
        if w == 0:
            swap.start()

    def first_stage(part, way, d):
        @pl.when(valid(way, d))
        def _():
            for piece in range(2):
                landed(part, way, d, piece)
                if d < n_out - 1:
                    pl.when(onward(way))(lambda: z_copy(part, way, d, piece).start())
                if piece == 0:
                    y_copy(part, way, d).start()
                    x_copy(part, way, d, 0).start()

    def second_stage(part, way, d):
        @pl.when(valid(way, d))
        def _():
            y_copy(part, way, d).wait_recv()
            x_copy(part, way, d, 1).start()

    order = [
        (part, way, d) for part in range(len(parts)) for d in range(1, n_out) for way in range(2)
    ]
    lag = 4
    for step in range(len(order) + lag):
        if step < len(order):
            first_stage(*order[step])
        if step >= lag:
            second_stage(*order[step - lag])
    for part, way, d in order:

        @pl.when(valid(way, d))
        def _():
            for piece in range(2):
                x_copy(part, way, d, piece).wait()
                if d < n_out - 1:
                    pl.when(onward(way))(lambda: z_copy(part, way, d, piece).wait_send())
            y_copy(part, way, d).wait_send()

    for part in range(len(parts)):
        y_own(part).wait()
        for way in range(2):

            @pl.when(onward(way))
            def _():
                z_copy(part, way, 0, 0).wait_send()
                z_copy(part, way, 0, 1).wait_send()

    swap.wait()


def gather_all(shards, by_rows, resid):
    members = lax.axis_size("fs")
    n_in = 2
    n_out = members // n_in
    count = len(shards)
    shapes = []
    for shard, rowwise in zip(shards, by_rows):
        rows, cols = shard.shape
        full = (rows * members, cols) if rowwise else (rows, cols * members)
        shapes.append(jax.ShapeDtypeStruct(full, shard.dtype))
    shapes.append(jax.ShapeDtypeStruct(resid.shape, resid.dtype))
    parts = []
    for w, shard in enumerate(shards):
        rows = shard.shape[0]
        pieces = 2 if w >= 4 else 1
        parts += [(w, piece * (rows // pieces), rows // pieces) for piece in range(pieces)]
    many = len(parts)
    pairs = [(many, 2, n_out, 2)] * 2 + [(many, 2, n_out)] * 2 + [(many, 2, n_out, 2)] * 2
    return pl.pallas_call(
        functools.partial(gather_kernel, by_rows, tuple(parts), n_out, n_in),
        out_shape=shapes,
        in_specs=[pl.BlockSpec(memory_space=pltpu.VMEM)] * (count + 1),
        out_specs=[pl.BlockSpec(memory_space=pl.ANY)] * (count + 1),
        scratch_shapes=[pltpu.SemaphoreType.DMA(pair) for pair in pairs]
        + [pltpu.SemaphoreType.DMA, pltpu.SemaphoreType.DMA, pltpu.SemaphoreType.DMA((count,))],
        compiler_params=pltpu.CompilerParams(
            collective_id=0, has_side_effects=True, vmem_limit_bytes=32 * 1024 * 1024
        ),
    )(*shards, resid)


def rms_norm(values, gain, width, power_sum):
    return values * lax.rsqrt(power_sum / width + 1e-06) * gain


def local(
    resid,
    gain_mix_in,
    u_weight,
    v_weight,
    u_scale,
    v_scale,
    v_gain,
    mix_matrix,
    mix_bias,
    out_weight,
    out_scale,
    gain_mix_out,
    gain_ffn_in,
    up_weight,
    up_scale,
    down_weight,
    down_scale,
    gain_ffn_out,
):
    rows = resid.shape[0]
    part_width = resid.shape[1]
    width = part_width * lax.axis_size("tp")
    lane = lax.axis_index("tp")
    full_rows = lax.all_gather(resid, "tp", axis=1, tiled=True)
    out_scales, down_scales = (
        lax.all_gather(out_scale, "fs", axis=0, tiled=True),
        lax.all_gather(down_scale, "fs", axis=0, tiled=True),
    )
    full_float = full_rows.astype(jnp.float32)
    normed = rms_norm(
        full_float, gain_mix_in, width, jnp.sum(full_float * full_float, axis=1, keepdims=True)
    ).astype(jnp.bfloat16)
    branch_cols = u_weight.shape[1]
    u_pre = jnp.dot(
        normed,
        lax.all_gather(u_weight.astype(jnp.bfloat16), "fs", axis=0, tiled=True),
        preferred_element_type=jnp.float32,
    )
    v_pre = jnp.dot(
        normed,
        lax.all_gather(v_weight.astype(jnp.bfloat16), "fs", axis=0, tiled=True),
        preferred_element_type=jnp.float32,
    )
    u_act = jax.nn.gelu(u_pre * u_scale)
    v_act = jax.nn.gelu(v_pre * v_scale)
    total, squares = lax.psum(
        (jnp.sum(v_act, axis=1, keepdims=True), jnp.sum(v_act * v_act, axis=1, keepdims=True)), "tp"
    )
    branch_width = branch_cols * lax.axis_size("tp")
    centre = total / branch_width
    spread = squares / branch_width - centre * centre
    v_norm = ((v_act - centre) * lax.rsqrt(spread + 1e-06) * v_gain).astype(jnp.bfloat16)
    groups = mix_matrix.shape[0]
    block = mix_matrix.shape[1]
    blocks = v_norm.reshape(rows // block, block, groups, branch_cols // groups)
    mixed = (
        jnp.einsum(
            "gts,bsgd->btgd",
            mix_matrix.astype(jnp.bfloat16),
            blocks,
            preferred_element_type=jnp.float32,
        )
        + mix_bias.T[None, :, :, None]
    )
    gated = (u_act * mixed.reshape(rows, branch_cols)).astype(jnp.bfloat16)
    partial_value = jnp.dot(
        gated,
        lax.all_gather(out_weight.astype(jnp.bfloat16), "fs", axis=1, tiled=True),
        preferred_element_type=jnp.float32,
    )
    mix_out = lax.psum(partial_value.astype(jnp.bfloat16), "tp").astype(jnp.float32) * out_scales
    power = jnp.sum(mix_out * mix_out, axis=1, keepdims=True)
    middle_full = (full_float + rms_norm(mix_out, gain_mix_out, width, power)).astype(jnp.bfloat16)
    middle = lax.dynamic_slice_in_dim(middle_full, lane * part_width, part_width, 1)
    middle_float = middle_full.astype(jnp.float32)
    ffn_in = rms_norm(
        middle_float,
        gain_ffn_in,
        width,
        jnp.sum(middle_float * middle_float, axis=1, keepdims=True),
    ).astype(jnp.bfloat16)
    up_half = up_weight.astype(jnp.bfloat16)
    down_half = down_weight.astype(jnp.bfloat16)
    whole_up = lax.all_gather(up_half, "fs", axis=0, tiled=True)
    raised = jnp.dot(ffn_in, whole_up, preferred_element_type=jnp.float32)
    hidden = jnp.square(jax.nn.relu(raised * up_scale)).astype(jnp.bfloat16)
    whole_down = lax.all_gather(down_half, "fs", axis=1, tiled=True)
    terms = jnp.dot(hidden, whole_down, preferred_element_type=jnp.float32)
    own_down = lax.dynamic_slice_in_dim(down_scales, lane * part_width, part_width, 0)
    ffn_out = (
        lax.psum_scatter(terms.astype(jnp.bfloat16), "tp", scatter_dimension=1, tiled=True).astype(
            jnp.float32
        )
        * own_down
    )
    power_out = lax.psum(jnp.sum(ffn_out * ffn_out, axis=1, keepdims=True), "tp")
    own_gain_out = lax.dynamic_slice_in_dim(gain_ffn_out, lane * part_width, part_width, 0)
    return (middle.astype(jnp.float32) + rms_norm(ffn_out, own_gain_out, width, power_out)).astype(
        jnp.bfloat16
    )


def local_fast(
    resid,
    gain_mix_in,
    u_weight,
    v_weight,
    u_scale,
    v_scale,
    v_gain,
    mix_matrix,
    mix_bias,
    out_weight,
    out_scale,
    gain_mix_out,
    gain_ffn_in,
    up_weight,
    up_scale,
    down_weight,
    down_scale,
    gain_ffn_out,
):
    rows = resid.shape[0]
    part_width = resid.shape[1]
    width = part_width * lax.axis_size("tp")
    lane = lax.axis_index("tp")
    half = jnp.bfloat16
    scale_cols = out_scale.shape[0]
    scales = jnp.concatenate(
        [jnp.broadcast_to(row, (16, scale_cols)) for row in (out_scale, down_scale)]
    )
    shards = [
        v_weight.astype(half),
        u_weight.astype(half),
        out_weight.astype(half),
        scales,
        up_weight.astype(half),
        down_weight.astype(half),
    ]
    whole_v, whole_u, whole_out, whole_scales, whole_up, whole_down, other = gather_all(
        shards, (True, True, False, True, True, False), resid
    )
    whole_scales = whole_scales.reshape(-1, 32, scale_cols)
    out_scales, down_scales = whole_scales[:, 0].reshape(-1), whole_scales[:, 16].reshape(-1)
    swap = [(0, 1), (1, 0)]
    full_rows = jnp.where(
        lane == 0,
        jnp.concatenate([resid, other], axis=1),
        jnp.concatenate([other, resid], axis=1),
    )
    full_float = full_rows.astype(jnp.float32)
    normed = rms_norm(
        full_float, gain_mix_in, width, jnp.sum(full_float * full_float, axis=1, keepdims=True)
    ).astype(jnp.bfloat16)
    branch_cols = u_weight.shape[1]
    u_pre = jnp.dot(
        normed,
        whole_u,
        preferred_element_type=jnp.float32,
    )
    v_pre = jnp.dot(
        normed,
        whole_v,
        preferred_element_type=jnp.float32,
    )
    u_act = jax.nn.gelu(u_pre * u_scale)
    v_act = jax.nn.gelu(v_pre * v_scale)
    total, squares = lax.psum(
        (jnp.sum(v_act, axis=1, keepdims=True), jnp.sum(v_act * v_act, axis=1, keepdims=True)), "tp"
    )
    branch_width = branch_cols * lax.axis_size("tp")
    centre = total / branch_width
    spread = squares / branch_width - centre * centre
    v_norm = ((v_act - centre) * lax.rsqrt(spread + 1e-06) * v_gain).astype(jnp.bfloat16)
    groups = mix_matrix.shape[0]
    block = mix_matrix.shape[1]
    blocks = v_norm.reshape(rows // block, block, groups, branch_cols // groups)
    mixed = (
        jnp.einsum(
            "gts,bsgd->btgd",
            mix_matrix.astype(jnp.bfloat16),
            blocks,
            preferred_element_type=jnp.float32,
        )
        + mix_bias.T[None, :, :, None]
    )
    gated = (u_act * mixed.reshape(rows, branch_cols)).astype(jnp.bfloat16)
    partial_value = jnp.dot(
        gated,
        whole_out,
        preferred_element_type=jnp.float32,
    )
    rounded = partial_value.astype(half)
    mix_out = (
        rounded.astype(jnp.float32) + lax.ppermute(rounded, "tp", swap).astype(jnp.float32)
    ) * out_scales
    power = jnp.sum(mix_out * mix_out, axis=1, keepdims=True)
    middle_full = (full_float + rms_norm(mix_out, gain_mix_out, width, power)).astype(jnp.bfloat16)
    middle = lax.dynamic_slice_in_dim(middle_full, lane * part_width, part_width, 1)
    middle_float = middle_full.astype(jnp.float32)
    ffn_in = rms_norm(
        middle_float,
        gain_ffn_in,
        width,
        jnp.sum(middle_float * middle_float, axis=1, keepdims=True),
    ).astype(jnp.bfloat16)
    raised = jnp.dot(ffn_in, whole_up, preferred_element_type=jnp.float32)
    hidden = jnp.square(jax.nn.relu(raised * up_scale)).astype(jnp.bfloat16)
    terms = jnp.dot(hidden, whole_down, preferred_element_type=jnp.float32)
    own_down = lax.dynamic_slice_in_dim(down_scales, lane * part_width, part_width, 0)
    terms = terms.astype(half)
    kept = lax.dynamic_slice_in_dim(terms, lane * part_width, part_width, 1)
    sent = lax.dynamic_slice_in_dim(terms, (1 - lane) * part_width, part_width, 1)
    ffn_out = (
        kept.astype(jnp.float32) + lax.ppermute(sent, "tp", swap).astype(jnp.float32)
    ) * own_down
    power_out = lax.psum(jnp.sum(ffn_out * ffn_out, axis=1, keepdims=True), "tp")
    own_gain_out = lax.dynamic_slice_in_dim(gain_ffn_out, lane * part_width, part_width, 0)
    return (middle.astype(jnp.float32) + rms_norm(ffn_out, own_gain_out, width, power_out)).astype(
        jnp.bfloat16
    )


def solution(mesh):
    in_specs = (
        P(("rep", "fs"), "tp"),
        P(),
        P("fs", "tp"),
        P("fs", "tp"),
        P("tp"),
        P("tp"),
        P("tp"),
        P("tp", None, None),
        P("tp", None),
        P("tp", "fs"),
        P("fs"),
        P(),
        P(),
        P("fs", "tp"),
        P("tp"),
        P("tp", "fs"),
        P("fs"),
        P(),
    )
    out_specs = P(("rep", "fs"), "tp")
    sizes = mesh.shape

    def whole(*args):
        columns = args[9].shape[1] // sizes["fs"]
        depth = args[2].shape[0] // sizes["fs"]
        paired = sizes["rep"] == 2 and sizes["tp"] == 2 and sizes["fs"] % 2 == 0
        fast = paired and columns % 128 == 0 and depth % 128 == 0
        return mapped(local_fast if fast else local)(*args)

    def mapped(body):
        return jax.shard_map(
            body, mesh=mesh, in_specs=in_specs, out_specs=out_specs, check_vma=False
        )

    return whole
```

profile of v0, /device:TPU:0, one launch (start us, length us, event | category | flops | bytes accessed | tf_op | source)
XLA Modules:
  0.0 327.2 jit_solution(1415180377804022923)
XLA Ops:
  0.0 1.2 convert_element_type.67.refs_1_
  1.2 2.0 convert_element_type.66.refs_0_
  3.2 1.8 convert_element_type.68.refs_2_
  5.0 1.7 convert_element_type.69.refs_4_
  6.7 0.0 copy-done.11
  6.7 1.1 convert_element_type.70.refs_5_
  7.8 0.0 copy-done.15
  7.8 0.0 copy-done.16
  7.8 0.0 copy-done
  7.9 0.0 copy-start.3
  7.9 1.2 copy-done.3
  9.1 0.9 copy-done.4
  10.0 0.9 copy-done.5
  11.0 216.9 %shard_map.172 = (bf16[2048,512]{1,0:T(8,128)(2,1)S(1)}, bf16[2048,512]{1,0:T(8,128)(2,1)S(1)}, bf16[512,2048]{1,0:T(8,128)(2,1)S(1)}, f32[256,256]{1,0:T(8,128)...) custom-call(bf16[256,512]{1,0:T(8,128)(2,1)S(1)} %copy-done.4, ...), custom_call_target="tpu_custom_call" | custom-call | tf_op jit(solution)/shard_map/pallas_call | solution.py:202
  227.9 0.0 copy-start.1
  227.9 0.0 copy-start.6
  227.9 0.0 copy-start.7
  227.9 0.0 copy-start.8
  228.0 0.0 copy-start.9
  228.0 1.5 fusion.3
  229.5 0.0 copy-done.17
  229.5 0.0 copy-done.20
  229.5 0.0 copy-start.14
  229.5 5.3 %fusion.50 = (f32[1024]{0:T(1024)S(1)}, f32[1024]{0:T(1024)S(1)}, f32[1024,512]{1,0:T(8,128)}) fusion(f32[512]{0:T(512)S(1)} %copy-done.20, bf16[2048,512]{1,0:T(8,128)(2,1)S(1)} %get-tuple-element.14, f32[2048]{0:T(1024)S(1)} %copy-done.17, f32[1024]{0:T(1024)S(1)} %add_rsqrt_fusion.4, bf16[1024,1024]{1,0:T(8,128)(2,1)S(1)} %copy-done, ...), kind=kOutput, calls=%fused_computation.64 | convolution fusion | flops 2181036032 | bytes 8411137 | tf_op jit(solution)/shard_map/dot_general | solution.py:380
  234.8 0.0 copy-done.1
  234.9 0.0 copy-start.13
  234.9 2.5 all-reduce
  237.4 1.9 multiply_convert_fusion.1
  239.4 2.1 reshape.48
  241.5 3.8 %bitcast_add_fusion = f32[8,128,8,64]{1,3,0,2:T(8,128)} fusion(bf16[8,128,8,64]{3,2,1,0:T(8,128)(2,1)} %reshape.48, f32[128,8]{0,1:T(8,128)S(1)} %bitcast.34, f32[8,128,128]{2,1,0:T(8,128)} %param.25), kind=kOutput, calls=%fused_computation.44 | convolution fusion | flops 134873088 | bytes 3674112 | tf_op jit(solution)/shard_map/gts,bsgd->btgd/dot_general | solution.py:398
  245.2 3.8 %copy.31 = f32[8,128,8,64]{3,2,1,0:T(8,128)} copy(f32[8,128,8,64]{1,3,0,2:T(8,128)} %bitcast_add_fusion) | data formatting | bytes 4194304 | tf_op jit(solution)/shard_map/reshape | solution.py:406
  249.0 4.8 %reshape.49 = f32[1024,512]{1,0:T(8,128)} reshape(f32[8,128,8,64]{3,2,1,0:T(8,128)} %copy.31) | data formatting | bytes 4194304 | tf_op jit(solution)/shard_map/reshape | solution.py:406
  253.9 10.1 %convolution_convert_fusion = bf16[1024,2048]{1,0:T(8,128)(2,1)} fusion(bf16[512,2048]{1,0:T(8,128)(2,1)} %copy-done.9, f32[1024,512]{1,0:T(8,128)} %reshape.49, bf16[2048,512]{1,0:T(8,128)(2,1)} %copy-done.8, f32[2048]{0:T(1024)S(1)} %copy-done.17, f32[1024]{0:T(1024)S(1)} %add_rsqrt_fusion.4, f32[512]{0:T(512)S(1)} %copy-done.21, ...), kind=kOutput, calls=%fused_computation.24 | convolution fusion | flops 4330094592 | bytes 14694401 | tf_op jit(solution)/shard_map/dot_general | solution.py:407
  263.9 0.2 collective-permute-start
  264.1 0.9 fusion.52
  265.0 6.5 %collective-permute-done = bf16[1024,2048]{1,0:T(8,128)(2,1)} collective-permute-done((bf16[1024,2048]{1,0:T(8,128)(2,1)}, bf16[1024,2048]{1,0:T(8,128)(2,1)}, u32[]{:S(2)}, u32[]{:S(2)}) %collective-permute-start) | collective-permute-done | bytes 4194336 | tf_op jit(solution)/shard_map/ppermute | solution.py:414
  271.4 5.3 %multiply_reduce_fusion = f32[1024]{0:T(1024)S(1)} fusion(bf16[1024,2048]{1,0:T(8,128)(2,1)} %collective-permute-done, bf16[1024,2048]{1,0:T(8,128)(2,1)} %convolution_convert_fusion, f32[2048]{0:T(1024)S(1)} %bitcast.25), kind=kLoop, calls=%fused_computation.13 | loop fusion | flops 12581888 | bytes 8400896 | tf_op jit(solution)/shard_map/reduce_sum | solution.py:416
  276.8 0.0 copy-start.18
  276.8 0.0 copy-start.19
  276.8 7.4 %fusion = (f32[1024]{0:T(1024)S(1)}, bf16[1024,2048]{1,0:T(8,128)(2,1)}) fusion(f32[2048]{0:T(1024)S(1)} %copy-done.12, f32[1024]{0:T(1024)S(1)} %add_rsqrt_fusion.2, f32[2048]{0:T(1024)S(1)} %bitcast.26, bf16[1024,2048]{1,0:T(8,128)(2,1)} %collective-permute-done, bf16[1024,2048]{1,0:T(8,128)(2,1)S(1)} %copy-done.10, bf16[1024,1024]{1,0:T(8,128)(2,1)S(1)} %copy-done, ...), kind=kLoop, calls=%fused_computation.5 | loop fusion | flops 44039168 | bytes 16801792 | tf_op jit(solution)/shard_map/reduce_sum | solution.py:424
  284.2 0.0 copy-done.19
  284.2 25.9 %fusion.16 = bf16[1024,2048]{1,0:T(8,128)(2,1)} fusion(bf16[2048,2048]{1,0:T(8,128)(2,1)} %get-tuple-element.18, bf16[2048,2048]{1,0:T(8,128)(2,1)} %copy-done.7, bf16[1024,2048]{1,0:T(8,128)(2,1)} %get-tuple-element.24, f32[2048]{0:T(1024)S(1)} %copy-done.18, f32[2048]{0:T(1024)S(1)} %copy-done.19, f32[1024]{0:T(1024)S(1)} %add_rsqrt_fusion.1), kind=kOutput, calls=%fused_computation.25 | convolution fusion | flops 17198743552 | bytes 25186304 | tf_op jit(solution)/shard_map/dot_general | solution.py:428
  310.1 3.1 constant_dynamic-slice_fusion
  313.2 0.2 collective-permute-start.1
  313.3 4.2 %collective-permute-done.1 = bf16[1024,1024]{1,0:T(8,128)(2,1)S(1)} collective-permute-done((bf16[1024,1024]{1,0:T(8,128)(2,1)}, bf16[1024,1024]{1,0:T(8,128)(2,1)S(1)}, u32[]{:S(2)}, u32[]{:S(2)}) %collective-permute-start.1) | collective-permute-done | bytes 2097184 | tf_op jit(solution)/shard_map/ppermute | solution.py:434
  317.5 2.5 multiply_reduce_fusion.1
  320.0 2.5 psum.23
  322.5 4.7 %add_convert_fusion = bf16[1024,1024]{1,0:T(8,128)(2,1)} fusion(bf16[1024,1024]{1,0:T(8,128)(2,1)S(1)} %collective-permute-done.1, f32[1024]{0:T(1024)S(1)} %dynamic-slice-done, f32[1024]{0:T(1024)S(1)} %bitcast.28, f32[1024]{0:T(1024)S(1)} %dynamic_slice.18, bf16[1024,2048]{1,0:T(8,128)(2,1)} %get-tuple-element.24, s32[]{:T(128)} %select_n.19, ...), kind=kLoop, calls=%fused_computation.17 | loop fusion | flops 9437184 | bytes 8400900 | tf_op jit(solution)/shard_map/convert_element_type | solution.py:438
  (34 shorter events, 0.1 us)
Async XLA Ops:
  0.0 6.7 %copy-start.11 = (f32[2048,256]{1,0:T(8,128)S(1)}, f32[2048,256]{1,0:T(8,128)}, u32[]{:S(2)}) copy-start(f32[2048,256]{1,0:T(8,128)} %param.33) | copy-start | bytes 6291460
  0.0 7.8 %copy-start.15 = (f32[256]{0:T(256)S(1)}, f32[256]{0:T(256)}, u32[]{:S(2)}) copy-start(f32[256]{0:T(256)} %param.28) | copy-start | bytes 3076
  0.0 7.8 %copy-start.16 = (f32[256]{0:T(256)S(1)}, f32[256]{0:T(256)}, u32[]{:S(2)}) copy-start(f32[256]{0:T(256)} %param.34) | copy-start | bytes 3076
  0.0 7.8 %copy-start = (bf16[1024,1024]{1,0:T(8,128)(2,1)S(1)}, bf16[1024,1024]{1,0:T(8,128)(2,1)}, u32[]{:S(2)}) copy-start(bf16[1024,1024]{1,0:T(8,128)(2,1)} %refs_6_.1) | copy-start | bytes 6291460
  7.9 1.2 copy-start.3
  9.1 0.9 copy-start.4
  10.0 0.9 copy-start.5
  11.0 218.5 %copy-start.17 = (f32[2048]{0:T(1024)S(1)}, f32[2048]{0:T(1024)}, u32[]{:S(2)}) copy-start(f32[2048]{0:T(1024)} %param.19) | copy-start | bytes 24580
  11.0 218.5 %copy-start.20 = (f32[512]{0:T(512)S(1)}, f32[512]{0:T(512)}, u32[]{:S(2)}) copy-start(f32[512]{0:T(512)} %param.23) | copy-start | bytes 6148
  227.9 6.9 %copy-start.1 = (bf16[1024,1024]{1,0:T(8,128)(2,1)}, bf16[1024,1024]{1,0:T(8,128)(2,1)S(1)}, u32[]{:S(2)}) copy-start(bf16[1024,1024]{1,0:T(8,128)(2,1)S(1)} %get-tuple-element.12) | copy-start | bytes 6291460
  227.9 6.9 %copy-start.6 = (f32[256,256]{1,0:T(8,128)}, f32[256,256]{1,0:T(8,128)S(1)}, u32[]{:S(2)}) copy-start(f32[256,256]{1,0:T(8,128)S(1)} %get-tuple-element.16) | copy-start | bytes 786436
  227.9 6.9 %copy-start.7 = (bf16[2048,2048]{1,0:T(8,128)(2,1)}, bf16[2048,2048]{1,0:T(8,128)(2,1)S(1)}, u32[]{:S(2)}) copy-start(bf16[2048,2048]{1,0:T(8,128)(2,1)S(1)} %get-tuple-element.17) | copy-start | bytes 25165828
  227.9 6.9 %copy-start.8 = (bf16[2048,512]{1,0:T(8,128)(2,1)}, bf16[2048,512]{1,0:T(8,128)(2,1)S(1)}, u32[]{:S(2)}) copy-start(bf16[2048,512]{1,0:T(8,128)(2,1)S(1)} %get-tuple-element.13) | copy-start | bytes 6291460
  228.0 6.9 %copy-start.9 = (bf16[512,2048]{1,0:T(8,128)(2,1)}, bf16[512,2048]{1,0:T(8,128)(2,1)S(1)}, u32[]{:S(2)}) copy-start(bf16[512,2048]{1,0:T(8,128)(2,1)S(1)} %get-tuple-element.15) | copy-start | bytes 6291460
  229.5 7.9 %copy-start.14 = (f32[512]{0:T(512)S(1)}, f32[512]{0:T(512)}, u32[]{:S(2)}) copy-start(f32[512]{0:T(512)} %param.24) | copy-start | bytes 6148
  234.9 6.6 %copy-start.13 = (f32[8,128]{1,0:T(8,128)S(1)}, f32[8,128]{1,0:T(8,128)}, u32[]{:S(2)}) copy-start(f32[8,128]{1,0:T(8,128)} %param.26) | copy-start | bytes 12292
  249.0 4.8 %copy-start.21 = (f32[512]{0:T(512)S(1)}, f32[512]{0:T(512)}, u32[]{:S(2)}) copy-start(f32[512]{0:T(512)} %param.22) | copy-start | bytes 6148
  263.9 7.5 %collective-permute-start = (bf16[1024,2048]{1,0:T(8,128)(2,1)}, bf16[1024,2048]{1,0:T(8,128)(2,1)}, u32[]{:S(2)}, u32[]{:S(2)}) collective-permute-start(bf16[1024,2048]{1,0:T(8,128)(2,1)} %convolution_convert_fusion), channel_id=1, source_target_pairs={{0,1},{1,0},{2,3},{3,2},{4,5},{5,4},{6,7},{7,6},{8,9},{9,8},{10,11... | collective-permute-start | bytes 12582920 | tf_op jit(solution)/shard_map/ppermute | solution.py:414
  271.4 5.3 %copy-start.2 = (bf16[1024,1024]{1,0:T(8,128)(2,1)S(1)}, bf16[1024,1024]{1,0:T(8,128)(2,1)}, u32[]{:S(2)}) copy-start(bf16[1024,1024]{1,0:T(8,128)(2,1)} %copy-done.1) | copy-start | bytes 6291460
  271.4 5.3 %copy-start.10 = (bf16[1024,2048]{1,0:T(8,128)(2,1)S(1)}, bf16[1024,2048]{1,0:T(8,128)(2,1)}, u32[]{:S(2)}) copy-start(bf16[1024,2048]{1,0:T(8,128)(2,1)} %convolution_convert_fusion) | copy-start | bytes 12582916
  271.4 5.3 %copy-start.12 = (f32[2048]{0:T(1024)S(1)}, f32[2048]{0:T(1024)}, u32[]{:S(2)}) copy-start(f32[2048]{0:T(1024)} %param.29) | copy-start | bytes 24580
  276.8 7.4 %copy-start.18 = (f32[2048]{0:T(1024)S(1)}, f32[2048]{0:T(1024)}, u32[]{:S(2)}) copy-start(f32[2048]{0:T(1024)} %param.32) | copy-start | bytes 24580
  276.8 7.4 %copy-start.19 = (f32[2048]{0:T(1024)S(1)}, f32[2048]{0:T(1024)}, u32[]{:S(2)}) copy-start(f32[2048]{0:T(1024)} %param.30) | copy-start | bytes 24580
  313.2 4.4 %collective-permute-start.1 = (bf16[1024,1024]{1,0:T(8,128)(2,1)}, bf16[1024,1024]{1,0:T(8,128)(2,1)S(1)}, u32[]{:S(2)}, u32[]{:S(2)}) collective-permute-start(bf16[1024,1024]{1,0:T(8,128)(2,1)} %constant_dynamic-slice_fusion), channel_id=1, source_target_pairs={{0,1},{1,0},{2,3},{3,2},{4,5},{5,4},{6,7},{7,6},{8,9},{9,8},{10,11... | collective-permute-start | bytes 6291464 | tf_op jit(solution)/shard_map/ppermute | solution.py:434
  313.3 9.2 %dynamic-slice-start = ((f32[2048]{0:T(1024)}, s32[]{:T(128)}), f32[1024]{0:T(1024)S(1)}, s32[]{:S(2)}) async-start(f32[2048]{0:T(1024)} %param.35, s32[]{:T(128)} %select_n.19), calls=%async_computation | async-start | bytes 8704 | tf_op jit(solution)/shard_map/dynamic_slice | solution.py:437
where the time goes:
time: 328 us; the launch traced here: 327 us
  Pallas kernels  217 us (66%)
  matrix products  45 us (14%)
  other arithmetic  31.2 us (10%)
  local copies, waits for them, and re-layouts  17.9 us (5%)
  waiting for transfers between devices  10.7 us (3%)
  blocking collectives  4.97 us (2%)
    pallas_call x1, Pallas kernels, gather_all(): pl.pallas_call(functools.partial(gather_kernel, by_rows, tuple(parts), n_...  217 us
    dot_general x1, matrix products, local_fast(): terms = jnp.dot(hidden, whole_down, preferred_element_type=jnp.float32)  25.9 us
    dot_general x1, matrix products, local_fast(): jnp.dot(gated, whole_out, preferred_element_type=jnp.float32)  10.1 us
    reshape x2, local copies, waits for them, and re-layouts, local_fast(): gated = (u_act * mixed.reshape(rows, branch_cols)).astype(jnp.bfloat16)  8.61 us
    reduce_sum x1, other arithmetic, local_fast(): jnp.sum(middle_float * middle_float, axis=1, keepdims=True)  7.37 us
  transfers between devices with their start and end apart: 2, of which 2 were waited for; matrix products, arithmetic and copies ran while one was open for 0% of the time, Pallas kernels for 0%

commit v1 on v0

v1 whole, which is shorter than its diff:
```python
import functools

import jax
import jax.numpy as jnp
from jax import lax
from jax.experimental import pallas as pl
from jax.experimental.pallas import tpu as pltpu
from jax.sharding import PartitionSpec as P


def fused_kernel(n_out, n_in, *refs):
    resid, v_weight, u_weight, out_weight, up_weight, down_weight = refs[:6]
    gain_mix_in, u_scale, v_scale, v_gain, mix_matrix, mix_bias = refs[6:12]
    out_scale, gain_mix_out, gain_ffn_in, up_scale, down_scale, gain_ffn_out = refs[12:18]
    result = refs[18]
    gathered, acc, x_buf, stream, h_buf, p_recv, f_recv, own_stat, mate_stat, mixers, bias = refs[
        19:30
    ]
    z_send, z_recv, y_send, y_recv, x_send, x_recv, load_sem = refs[30:37]
    t_send, t_recv, c_send, c_recv, out_sem = refs[37:42]
    half, single = jnp.bfloat16, jnp.float32
    parts, members, depth, branch = gathered.shape
    rows, width = acc.shape
    part = width // 2
    pieces = branch // depth
    n_ffn = (parts - 3) // 2
    groups, block = mix_matrix.shape[0], mix_matrix.shape[1]
    chunk = rows // n_out
    member = lax.axis_index("fs")
    rep = lax.axis_index("rep")
    tp = lax.axis_index("tp")
    outer, inner = member // n_in, member % n_in
    peer_in = 1 - inner
    has_left, has_right = outer > 0, outer < n_out - 1
    across, twin, mate = {"fs": outer * n_in + peer_in}, {"rep": 1 - rep}, {"tp": 1 - tp}

    def greet(device):
        pl.semaphore_signal(barrier, inc=1, device_id=device, device_id_type=pl.DeviceIdType.MESH)

    barrier = pltpu.get_barrier_semaphore()
    for step in (1, n_out - 1):
        greet({"fs": lax.rem(outer + step, n_out) * n_in + inner})
    for device in (across, twin, mate):
        greet(device)

    def remote(src, dst, send, recv, device):
        return pltpu.make_async_remote_copy(
            src_ref=src,
            dst_ref=dst,
            send_sem=send,
            recv_sem=recv,
            device_id=device,
            device_id_type=pl.DeviceIdType.MESH,
        )

    def slot(p, index, base, size):
        return gathered.at[p, index, pl.ds(pl.multiple_of(base, depth // 8), size), :]

    def moved(ref, send, recv, device):
        return remote(ref, ref, send, recv, device)

    def z_copy(p, src, right):
        ref = slot(p, src * n_in + inner, rep * (depth // 4), 3 * depth // 4)
        way = right.astype(jnp.int32)
        device = {"fs": (outer + 2 * way - 1) * n_in + inner}
        return moved(ref, z_send.at[p, way, src], z_recv.at[p, src], device)

    def y_copy(p, src):
        ref = slot(p, src * n_in + inner, rep * (depth // 2), depth // 2)
        return moved(ref, y_send.at[p, src], y_recv.at[p, src], across)

    def y_own(p):
        ref = slot(p, member, rep * (depth // 8), 7 * depth // 8)
        return moved(ref, y_send.at[p, outer], y_recv.at[p, outer], across)

    def x_own(p):
        ref = slot(p, outer * n_in + peer_in, rep * (7 * depth // 8), depth // 8)
        return moved(ref, x_send.at[p, outer, 0], x_recv.at[p, outer, 0], twin)

    def x_side(p, src):
        ref = slot(p, src * n_in + inner, rep * (3 * depth // 4), depth // 4)
        return moved(ref, x_send.at[p, src, 0], x_recv.at[p, src, 0], twin)

    def x_diag(p, src):
        ref = slot(p, src * n_in + peer_in, rep * (depth // 2), depth // 2)
        return moved(ref, x_send.at[p, src, 1], x_recv.at[p, src, 1], twin)

    def source(k):
        both = jnp.minimum(outer, n_out - 1 - outer)
        near = k <= 2 * both
        d = jnp.where(near, (k + 1) // 2, k - both)
        long_right = outer < n_out - 1 - outer
        right = jnp.where(near, k % 2 == 0, long_right)
        return jnp.where(right, outer + d, outer - d)

    yes = outer >= 0

    def own_start(p):
        pl.when(has_right)(lambda: z_copy(p, outer, yes).start())
        pl.when(has_left)(lambda: z_copy(p, outer, outer < 0).start())
        y_own(p).start()

    def own_finish(p):
        y_own(p).wait_recv()
        x_own(p).start()

    def onward(src):
        return jnp.where(src < outer, has_right, has_left)

    def first_stage(p, k):
        src = source(k)
        z_copy(p, src, src < outer).wait_recv()
        pl.when(onward(src))(lambda: z_copy(p, src, src < outer).start())
        y_copy(p, src).start()
        x_side(p, src).start()

    def second_stage(p, k):
        src = source(k)
        y_copy(p, src).wait_recv()
        x_diag(p, src).start()

    lag = 2
    others = n_out - 1

    def comm(p, k):
        @pl.when(k == 0)
        def _():
            pl.when(p + 2 < parts)(lambda: own_start(p + 2))
            own_finish(p)

        @pl.when(k > 0)
        def _():
            first_stage(p, k)
            late = p * others + k - 1 - lag
            pl.when(late >= 0)(lambda: second_stage(late // others, late % others + 1))

    def finish(p):
        x_own(p).wait_recv()

        @pl.loop(1, n_out)
        def _(k):
            src = source(k)
            x_side(p, src).wait_recv()
            x_diag(p, src).wait_recv()

    def drain():
        @pl.loop(0, parts)
        def _(p):
            pl.when(has_right)(lambda: z_copy(p, outer, yes).wait_send())
            pl.when(has_left)(lambda: z_copy(p, outer, outer < 0).wait_send())
            y_own(p).wait_send()
            x_own(p).wait_send()

            @pl.loop(1, n_out)
            def _(k):
                src = source(k)
                pl.when(onward(src))(lambda: z_copy(p, src, src < outer).wait_send())
                y_copy(p, src).wait_send()
                x_side(p, src).wait_send()
                x_diag(p, src).wait_send()

    def tile(p):
        return pl.ds((p % n_out) * depth, depth), (p // n_out) * branch

    def loads(p):
        low, left = tile(p)
        if p < 2 or 3 <= p < 3 + n_ffn:
            src = (v_weight, u_weight)[p] if p < 2 else up_weight
            first = 0 if p < 2 else (p - 3) * branch
            return [
                pltpu.make_async_copy(
                    src.at[:, pl.ds(first, branch)],
                    acc.at[low, pl.ds(left, branch)],
                    load_sem.at[p, 0],
                )
            ]
        src, first = (out_weight, 0) if p == 2 else (down_weight, (p - 3 - n_ffn) * branch)
        return [
            pltpu.make_async_copy(
                src.at[pl.ds(first + i * depth, depth), :],
                acc.at[low, pl.ds(left + i * depth, depth)],
                load_sem.at[p, i],
            )
            for i in range(pieces)
        ]

    def cast(p):
        for copy in loads(p):
            copy.wait()
        low, left = tile(p)
        if p < 2 or 3 <= p < 3 + n_ffn:
            gathered[p, member] = acc[low, pl.ds(left, branch)].astype(half)
            return
        scale = (out_scale if p == 2 else down_scale)[...]
        for i in range(pieces):
            values = acc[low, pl.ds(left + i * depth, depth)] * scale
            gathered[p, member, :, pl.ds(i * depth, depth)] = values.astype(half)

    for p in (0, 1):
        for copy in loads(p):
            copy.start()
    fetch = pltpu.make_async_copy(resid, stream.at[tp], out_sem.at[0])
    fetch.start()
    for p in range(2, parts):
        for copy in loads(p):
            copy.start()
    cast(0)
    cast(1)
    swap = remote(stream.at[tp], stream.at[tp], t_send.at[0], t_recv.at[0], mate)
    pl.semaphore_wait(barrier, 5)
    own_start(0)
    own_start(1)
    fetch.wait()
    swap.start()
    for p in range(2, parts):
        cast(p)
    mixers[...] = mix_matrix[...].reshape(groups * block, block).astype(half)
    span = branch // groups
    turned = mix_bias[...].T
    lanes = lax.broadcasted_iota(jnp.int32, (block, 128), 1)
    for first in range(0, branch, 128):
        column = turned[:, first // span : first // span + 1]
        level = jnp.broadcast_to(column, (block, 128))
        for g in range(first // span + 1, (first + 127) // span + 1):
            level = jnp.where(lanes >= g * span - first, turned[:, g : g + 1], level)
        bias[:, pl.ds(first, 128)] = level
    swap.wait()

    def here(k):
        return pl.ds(pl.multiple_of(k * chunk, chunk), chunk)

    def dot(a, b):
        return jnp.dot(a, b, preferred_element_type=single)

    def spanned(p):
        return gathered[p].reshape(width, branch)

    def norm_stage(k):
        r = here(k)
        a, b = stream[0, r, :].astype(single), stream[1, r, :].astype(single)
        power = jnp.sum(a * a, axis=1, keepdims=True) + jnp.sum(b * b, axis=1, keepdims=True)
        scale = lax.rsqrt(power / width + 1e-06)
        x_buf[r, pl.ds(0, part)] = (a * scale * gain_mix_in[:, :part]).astype(half)
        x_buf[r, pl.ds(part, part)] = (b * scale * gain_mix_in[:, part:]).astype(half)

    def v_stage(k):
        r = here(k)
        act = jax.nn.gelu(dot(x_buf[r, :], spanned(0)) * v_scale[...])
        acc[r, pl.ds(0, branch)] = act
        total = jnp.sum(act, axis=1, keepdims=True)
        squares = jnp.sum(act * act, axis=1, keepdims=True)
        lane = lax.broadcasted_iota(jnp.int32, (chunk, 128), 1)
        own_stat[r, :] = jnp.where(lane == 0, total, squares)

    stat_copy = remote(own_stat, mate_stat.at[0], t_send.at[1], t_recv.at[1], mate)

    def u_stage(k):
        pl.when(k == 0)(lambda: stat_copy.start())
        r = here(k)
        act = jax.nn.gelu(dot(x_buf[r, :], spanned(1)) * u_scale[...])
        acc[r, pl.ds(branch, branch)] = act

    def p_copy(k):
        r = here(k)
        return remote(h_buf.at[r, :], p_recv.at[r, :], c_send.at[k, 0], c_recv.at[k, 0], mate)

    def times(values, p, m):
        total = dot(values[:, :depth], gathered[p, m, :, pl.ds(0, depth)])
        for i in range(1, pieces):
            total += dot(
                values[:, i * depth : (i + 1) * depth], gathered[p, m, :, pl.ds(i * depth, depth)]
            )
        return total

    def out_stage(k):
        pl.when(k == 0)(lambda: stat_copy.wait())
        pl.when(k > 0)(lambda: p_copy(k - 1).start())
        r = here(k)
        sums = own_stat[r, :] + mate_stat[0, r, :]
        centre = sums[:, 0:1] / (2 * branch)
        spread = sums[:, 1:2] / (2 * branch) - centre * centre
        scale = lax.rsqrt(spread + 1e-06)
        normed = ((acc[r, pl.ds(0, branch)] - centre) * scale * v_gain[...]).astype(half)
        per = 256 // span
        lane = lax.broadcasted_iota(jnp.int32, (block, 256), 1)
        gates = []
        for b in range(chunk // block):
            line = []
            for q in range(branch // 256):
                both = dot(
                    mixers[pl.ds(q * per * block, per * block), :],
                    normed[b * block : (b + 1) * block, q * 256 : (q + 1) * 256],
                )
                mixed = both[:block]
                for g in range(1, per):
                    mixed = jnp.where(lane >= g * span, both[g * block : (g + 1) * block], mixed)
                line.append(mixed + bias[:, pl.ds(q * 256, 256)])
            gates.append(jnp.concatenate(line, axis=1))
        gate = jnp.concatenate(gates, axis=0)
        gated = (acc[r, pl.ds(branch, branch)] * gate).astype(half)
        for m in range(members):
            h_buf[r, pl.ds(m * depth, depth)] = times(gated, 2, m).astype(half)

    def mid_stage(k):
        pl.when(k == 0)(lambda: p_copy(n_out - 1).start())
        p_copy(k).wait()
        r = here(k)
        mix = h_buf[r, :].astype(single) + p_recv[r, :].astype(single)
        scale = lax.rsqrt(jnp.sum(mix * mix, axis=1, keepdims=True) / width + 1e-06)
        mix = mix * scale * gain_mix_out[...]
        a = (stream[0, r, :].astype(single) + mix[:, :part]).astype(half)
        b = (stream[1, r, :].astype(single) + mix[:, part:]).astype(half)
        stream[0, r, :] = a
        stream[1, r, :] = b
        a, b = a.astype(single), b.astype(single)
        power = jnp.sum(a * a, axis=1, keepdims=True) + jnp.sum(b * b, axis=1, keepdims=True)
        scale = lax.rsqrt(power / width + 1e-06)
        x_buf[r, pl.ds(0, part)] = (a * scale * gain_ffn_in[:, :part]).astype(half)
        x_buf[r, pl.ds(part, part)] = (b * scale * gain_ffn_in[:, part:]).astype(half)

    def strip(j):
        return pl.ds(pl.multiple_of(j * branch, branch), branch)

    def up_stage(k, p):
        r, cols = here(k), strip(p - 3)
        raised = jax.nn.relu(dot(x_buf[r, :], spanned(p)) * up_scale[:, cols])
        h_buf[r, cols] = (raised * raised).astype(half)

    def down_stage(k, p, fresh):
        r = here(k)
        values = h_buf[r, strip(p - 3 - n_ffn)]
        for m in range(members):
            cols = pl.ds(m * depth, depth)
            terms = times(values, p, m)
            acc[r, cols] = terms if fresh else acc[r, cols] + terms

    def segment(p, needs, *stages):
        @pl.loop(0, n_out)
        def _(k):
            comm(p, k)
            if needs is not None:
                pl.when(k == 0)(lambda: finish(needs))
            for stage in stages:
                stage(k)

    segment(0, None)
    segment(1, None, norm_stage)
    segment(2, 0, v_stage)
    segment(3, 1, u_stage)
    segment(4, 2, out_stage)
    segment(5, 3, mid_stage, lambda k: up_stage(k, 3))

    @pl.loop(6, 5 + n_ffn)
    def _(p):
        segment(p, p - 2, lambda k: up_stage(k, p - 2))

    for p in range(5 + n_ffn, parts):
        segment(p, p - 2, lambda k: down_stage(k, p - 2, p == 5 + n_ffn))
    last = parts - 1
    for late in range(parts * others - lag, parts * others):
        second_stage(late // others, late % others + 1)

    finish(last - 1)

    @pl.loop(0, n_out)
    def _(k):
        down_stage(k, last - 1, False)

    finish(last)
    share = members // 2

    def f_copy(k):
        r = here(k)
        return remote(
            x_buf.at[r, pl.ds(0, part)], f_recv.at[r, :], c_send.at[k, 1], c_recv.at[k, 1], mate
        )

    def s_copy(k):
        r = here(k)
        return remote(
            own_stat.at[r, :], mate_stat.at[1, r, :], c_send.at[k, 0], c_recv.at[k, 0], mate
        )

    def own_cols(m):
        return pl.ds(pl.multiple_of(m * depth, depth), depth)

    @pl.loop(0, n_out)
    def _(k):
        r = here(k)
        values = h_buf[r, pl.ds((n_ffn - 1) * branch, branch)]
        for i in range(share):
            m = (1 - tp) * share + i
            terms = acc[r, own_cols(m)] + times(values, last, m)
            x_buf[r, pl.ds(i * depth, depth)] = terms.astype(half)
        pl.when(k > 0)(lambda: f_copy(k - 1).start())

    f_copy(n_out - 1).start()

    @pl.loop(0, n_out)
    def _(k):
        r = here(k)
        values = h_buf[r, pl.ds((n_ffn - 1) * branch, branch)]
        kept = []
        for i in range(share):
            m = tp * share + i
            terms = acc[r, own_cols(m)] + times(values, last, m)
            kept.append(terms.astype(half).astype(single))
        f_copy(k).wait()
        power = jnp.zeros((chunk, 1), single)
        for i in range(share):
            total = kept[i] + f_recv[r, pl.ds(i * depth, depth)].astype(single)
            power += jnp.sum(total * total, axis=1, keepdims=True)
            acc[r, own_cols(tp * share + i)] = total
        own_stat[r, :] = jnp.broadcast_to(power, (chunk, 128))
        pl.when(k > 0)(lambda: s_copy(k - 1).start())

    s_copy(n_out - 1).start()
    drain()

    def leave(k):
        r = here(k)
        return pltpu.make_async_copy(
            x_buf.at[r, pl.ds(part, part)], result.at[r, :], out_sem.at[k]
        )

    @pl.loop(0, n_out)
    def _(k):
        s_copy(k).wait()
        r = here(k)
        power = own_stat[r, 0:1] + mate_stat[1, r, 0:1]
        scale = lax.rsqrt(power / width + 1e-06)
        cols = pl.ds(pl.multiple_of(tp * part, part), part)
        total = acc[r, cols] * scale * gain_ffn_out[:, cols]
        x_buf[r, pl.ds(part, part)] = (stream[tp, r, :].astype(single) + total).astype(half)
        leave(k).start()

    for k in range(n_out):
        leave(k).wait()


def rms_norm(values, gain, width, power_sum):
    return values * lax.rsqrt(power_sum / width + 1e-06) * gain


def local(
    resid,
    gain_mix_in,
    u_weight,
    v_weight,
    u_scale,
    v_scale,
    v_gain,
    mix_matrix,
    mix_bias,
    out_weight,
    out_scale,
    gain_mix_out,
    gain_ffn_in,
    up_weight,
    up_scale,
    down_weight,
    down_scale,
    gain_ffn_out,
):
    rows = resid.shape[0]
    part_width = resid.shape[1]
    width = part_width * lax.axis_size("tp")
    lane = lax.axis_index("tp")
    full_rows = lax.all_gather(resid, "tp", axis=1, tiled=True)
    out_scales, down_scales = (
        lax.all_gather(out_scale, "fs", axis=0, tiled=True),
        lax.all_gather(down_scale, "fs", axis=0, tiled=True),
    )
    full_float = full_rows.astype(jnp.float32)
    normed = rms_norm(
        full_float, gain_mix_in, width, jnp.sum(full_float * full_float, axis=1, keepdims=True)
    ).astype(jnp.bfloat16)
    branch_cols = u_weight.shape[1]
    u_pre = jnp.dot(
        normed,
        lax.all_gather(u_weight.astype(jnp.bfloat16), "fs", axis=0, tiled=True),
        preferred_element_type=jnp.float32,
    )
    v_pre = jnp.dot(
        normed,
        lax.all_gather(v_weight.astype(jnp.bfloat16), "fs", axis=0, tiled=True),
        preferred_element_type=jnp.float32,
    )
    u_act = jax.nn.gelu(u_pre * u_scale)
    v_act = jax.nn.gelu(v_pre * v_scale)
    total, squares = lax.psum(
        (jnp.sum(v_act, axis=1, keepdims=True), jnp.sum(v_act * v_act, axis=1, keepdims=True)), "tp"
    )
    branch_width = branch_cols * lax.axis_size("tp")
    centre = total / branch_width
    spread = squares / branch_width - centre * centre
    v_norm = ((v_act - centre) * lax.rsqrt(spread + 1e-06) * v_gain).astype(jnp.bfloat16)
    groups = mix_matrix.shape[0]
    block = mix_matrix.shape[1]
    blocks = v_norm.reshape(rows // block, block, groups, branch_cols // groups)
    mixed = (
        jnp.einsum(
            "gts,bsgd->btgd",
            mix_matrix.astype(jnp.bfloat16),
            blocks,
            preferred_element_type=jnp.float32,
        )
        + mix_bias.T[None, :, :, None]
    )
    gated = (u_act * mixed.reshape(rows, branch_cols)).astype(jnp.bfloat16)
    partial_value = jnp.dot(
        gated,
        lax.all_gather(out_weight.astype(jnp.bfloat16), "fs", axis=1, tiled=True),
        preferred_element_type=jnp.float32,
    )
    mix_out = lax.psum(partial_value.astype(jnp.bfloat16), "tp").astype(jnp.float32) * out_scales
    power = jnp.sum(mix_out * mix_out, axis=1, keepdims=True)
    middle_full = (full_float + rms_norm(mix_out, gain_mix_out, width, power)).astype(jnp.bfloat16)
    middle = lax.dynamic_slice_in_dim(middle_full, lane * part_width, part_width, 1)
    middle_float = middle_full.astype(jnp.float32)
    ffn_in = rms_norm(
        middle_float,
        gain_ffn_in,
        width,
        jnp.sum(middle_float * middle_float, axis=1, keepdims=True),
    ).astype(jnp.bfloat16)
    up_half = up_weight.astype(jnp.bfloat16)
    down_half = down_weight.astype(jnp.bfloat16)
    whole_up = lax.all_gather(up_half, "fs", axis=0, tiled=True)
    raised = jnp.dot(ffn_in, whole_up, preferred_element_type=jnp.float32)
    hidden = jnp.square(jax.nn.relu(raised * up_scale)).astype(jnp.bfloat16)
    whole_down = lax.all_gather(down_half, "fs", axis=1, tiled=True)
    terms = jnp.dot(hidden, whole_down, preferred_element_type=jnp.float32)
    own_down = lax.dynamic_slice_in_dim(down_scales, lane * part_width, part_width, 0)
    ffn_out = (
        lax.psum_scatter(terms.astype(jnp.bfloat16), "tp", scatter_dimension=1, tiled=True).astype(
            jnp.float32
        )
        * own_down
    )
    power_out = lax.psum(jnp.sum(ffn_out * ffn_out, axis=1, keepdims=True), "tp")
    own_gain_out = lax.dynamic_slice_in_dim(gain_ffn_out, lane * part_width, part_width, 0)
    return (middle.astype(jnp.float32) + rms_norm(ffn_out, own_gain_out, width, power_out)).astype(
        jnp.bfloat16
    )


def local_fast(
    resid,
    gain_mix_in,
    u_weight,
    v_weight,
    u_scale,
    v_scale,
    v_gain,
    mix_matrix,
    mix_bias,
    out_weight,
    out_scale,
    gain_mix_out,
    gain_ffn_in,
    up_weight,
    up_scale,
    down_weight,
    down_scale,
    gain_ffn_out,
):
    rows, part = resid.shape
    members = lax.axis_size("fs")
    width = part * 2
    depth, branch = v_weight.shape
    hidden = up_weight.shape[1]
    parts = 3 + 2 * (hidden // branch)
    n_in = 2
    n_out = members // n_in
    half, single = jnp.bfloat16, jnp.float32
    groups, block = mix_matrix.shape[0], mix_matrix.shape[1]

    def row(vector):
        return vector.reshape(1, -1)

    big = [resid, v_weight, u_weight, out_weight, up_weight, down_weight]
    small = [
        row(gain_mix_in),
        row(u_scale),
        row(v_scale),
        row(v_gain),
        mix_matrix,
        mix_bias,
        row(out_scale),
        row(gain_mix_out),
        row(gain_ffn_in),
        row(up_scale),
        row(down_scale),
        row(gain_ffn_out),
    ]
    dma = pltpu.SemaphoreType.DMA
    scratch = [
        pltpu.VMEM((parts, members, depth, branch), half),
        pltpu.VMEM((rows, width), single),
        pltpu.VMEM((rows, width), half),
        pltpu.VMEM((2, rows, part), half),
        pltpu.VMEM((rows, width), half),
        pltpu.VMEM((rows, width), half),
        pltpu.VMEM((rows, part), half),
        pltpu.VMEM((rows, 128), single),
        pltpu.VMEM((2, rows, 128), single),
        pltpu.VMEM((groups * block, block), half),
        pltpu.VMEM((block, branch), single),
        dma((parts, 2, n_out)),
        dma((parts, n_out)),
        dma((parts, n_out)),
        dma((parts, n_out)),
        dma((parts, n_out, 2)),
        dma((parts, n_out, 2)),
        dma((parts, branch // depth)),
        dma((2,)),
        dma((2,)),
        dma((n_out, 2)),
        dma((n_out, 2)),
        dma((n_out,)),
    ]
    return pl.pallas_call(
        functools.partial(fused_kernel, n_out, n_in),
        out_shape=jax.ShapeDtypeStruct((rows, part), half),
        in_specs=[pl.BlockSpec(memory_space=pl.ANY)] * len(big)
        + [pl.BlockSpec(memory_space=pltpu.VMEM)] * len(small),
        out_specs=pl.BlockSpec(memory_space=pl.ANY),
        scratch_shapes=scratch,
        compiler_params=pltpu.CompilerParams(
            collective_id=0, has_side_effects=True, vmem_limit_bytes=63 * 1024 * 1024
        ),
        name="fused_layer",
    )(*big, *small)


def solution(mesh):
    in_specs = (
        P(("rep", "fs"), "tp"),
        P(),
        P("fs", "tp"),
        P("fs", "tp"),
        P("tp"),
        P("tp"),
        P("tp"),
        P("tp", None, None),
        P("tp", None),
        P("tp", "fs"),
        P("fs"),
        P(),
        P(),
        P("fs", "tp"),
        P("tp"),
        P("tp", "fs"),
        P("fs"),
        P(),
    )
    out_specs = P(("rep", "fs"), "tp")
    sizes = mesh.shape

    def whole(*args):
        rows = args[0].shape[0] // (sizes["rep"] * sizes["fs"])
        width = args[0].shape[1]
        branch = args[2].shape[1] // sizes["tp"]
        hidden = args[13].shape[1] // sizes["tp"]
        groups, block = args[7].shape[0] // sizes["tp"], args[7].shape[1]
        planes, depth = sizes["fs"] // 2, width // sizes["fs"]
        paired = sizes["rep"] == 2 and sizes["tp"] == 2 and sizes["fs"] % 4 == 0
        fits = depth % 256 == 0 and branch % depth == 0 and hidden % branch == 0
        blocks = rows % (planes * block) == 0 and (256 * groups) % branch == 0
        small = 2 * width * (3 * branch + 2 * hidden) <= 24 * 1024 * 1024
        fast = paired and planes >= 2 and fits and blocks and small
        return mapped(local_fast if fast else local)(*args)

    def mapped(body):
        return jax.shard_map(
            body, mesh=mesh, in_specs=in_specs, out_specs=out_specs, check_vma=False
        )

    return whole
```

time: 328 us -> 189 us (0.58)
  matrix products: 45 us -> 0 us
  other arithmetic: 31.2 us -> 0 us
  Pallas kernels: 217 us -> 186 us
  local copies, waits for them, and re-layouts: 17.9 us -> 3.08 us
  waiting for transfers between devices: 10.7 us -> 0 us
  blocking collectives: 4.97 us -> 0 us
    dot_general x4 -> x0, matrix products: 45 us -> none  [the longest x1 25.9 us: local_fast(): terms = jnp.dot(hidden, whole_down, preferred_element_type=jnp.float32)]
    pallas_call x1, Pallas kernels: 217 us -> 186 us  [local_fast(): pl.pallas_call(functools.partial(fused_kernel, n_out, n_in), out_shape=ja...]
    reduce_sum x4 -> x0, other arithmetic: 16.6 us -> none  [the longest x1 7.37 us: local_fast(): jnp.sum(middle_float * middle_float, axis=1, keepdims=True)]
    convert_element_type x7 -> x0, other arithmetic: 14.4 us -> none  [the longest x1 4.72 us: local_fast(): (middle.astype(jnp.float32) + rms_norm(ffn_out, own_gain_out, width, powe...]
    reshape x3 -> x0, local copies, waits for them, and re-layouts: 10.7 us -> none  [the longest x2 8.61 us: local_fast(): gated = (u_act * mixed.reshape(rows, branch_cols)).astype(jnp.bfloat16)]
    ppermute x2 -> x0, waiting for transfers between devices: 10.7 us -> none  [the longest x1 6.45 us: local_fast(): lax.ppermute(rounded, 'tp', swap).astype(jnp.float32)]
    psum x2 -> x0, blocking collectives: 4.97 us -> none  [the longest x1 2.5 us: local_fast(): lax.psum((jnp.sum(v_act, axis=1, keepdims=True), jnp.sum(v_act * v_act, a...]
  transfers between devices with their start and end apart: 2 -> 0, of which waited for: 2 -> 0; matrix products, arithmetic and copies ran while one was open for 0% -> 0% of each run, Pallas kernels for 0% -> 0%
where the time goes in v1:
time: 189 us
  Pallas kernels  186 us (98%)
  local copies, waits for them, and re-layouts  3.08 us (2%)
    pallas_call x1, Pallas kernels, local_fast(): pl.pallas_call(functools.partial(fused_kernel, n_out, n_in), out_shape=ja...  186 us

profile of v1, /device:TPU:0, one launch (start us, length us, event | category | flops | bytes accessed | tf_op | source)
XLA Modules:
  0.0 188.6 jit_solution(15239417401321498659)
XLA Ops:
  0.0 185.5 %fused_layer.1 = bf16[1024,1024]{1,0:T(8,128)(2,1)} custom-call(bf16[1024,1024]{1,0:T(8,128)(2,1)} %refs_0_.1, f32[256,512]{1,0:T(8,128)} %refs_1_.1, f32[256,512]{1,0:T(8,128)} %refs_2_.1, f32[512,256]{1,0:T(8,128)} %refs_3_.1, f32[256,2048]{1,0:T(8,128)} %refs_4_.1, f32[2048,256]{1,0:T(8,128)} %refs_5_.1, f32[1,2048]{1,0:T(1,128)} %bitcast.10, ...), custom_call_target="tpu_custom_call" | custom-call | tf_op jit(solution)/shard_map/fused_layer/pallas_call | solution.py:623
  185.6 3.1 %copy.20 = bf16[1024,1024]{1,0:T(8,128)(2,1)} copy(bf16[1024,1024]{1,0:T(8,128)(2,1)} %fused_layer.1) | data formatting | bytes 4194304

commit v2 on v1

--- a/solution.py
+++ b/solution.py
@@ -13,15 +13,17 @@
     gain_mix_in, u_scale, v_scale, v_gain, mix_matrix, mix_bias = refs[6:12]
     out_scale, gain_mix_out, gain_ffn_in, up_scale, down_scale, gain_ffn_out = refs[12:18]
     result = refs[18]
-    gathered, acc, x_buf, stream, h_buf, p_recv, f_recv, own_stat, mate_stat, mixers, bias = refs[
-        19:30
+    gathered, acc, x_buf, x_twin, stream, h_buf, terms, p_recv, d_recv, o_recv = refs[19:29]
+    own_stat, mate_stat, mixers, bias = refs[29:33]
+    z_send, z_recv, e_send, e_recv, y_send, y_recv, x_send, x_recv, load_sem = refs[33:42]
+    t_send, t_recv, c_send, c_recv, a_send, a_recv, d_send, d_sem, o_send, o_sem, out_sem = refs[
+        42:53
     ]
-    z_send, z_recv, y_send, y_recv, x_send, x_recv, load_sem = refs[30:37]
-    t_send, t_recv, c_send, c_recv, out_sem = refs[37:42]
     half, single = jnp.bfloat16, jnp.float32
     parts, members, depth, branch = gathered.shape
-    rows, width = acc.shape
+    rows, width = x_buf.shape
     part = width // 2
+    shared = h_buf.shape[2]
     pieces = branch // depth
     n_ffn = (parts - 3) // 2
     groups, block = mix_matrix.shape[0], mix_matrix.shape[1]
@@ -31,6 +33,7 @@
     tp = lax.axis_index("tp")
     outer, inner = member // n_in, member % n_in
     peer_in = 1 - inner
+    cut = 3 * depth // 16
     has_left, has_right = outer > 0, outer < n_out - 1
     across, twin, mate = {"fs": outer * n_in + peer_in}, {"rep": 1 - rep}, {"tp": 1 - tp}
 
@@ -54,23 +57,33 @@
         )
 
     def slot(p, index, base, size):
-        return gathered.at[p, index, pl.ds(pl.multiple_of(base, depth // 8), size), :]
+        return gathered.at[p, index, pl.ds(pl.multiple_of(base, depth // 16), size), :]
 
     def moved(ref, send, recv, device):
         return remote(ref, ref, send, recv, device)
 
     def z_copy(p, src, right):
-        ref = slot(p, src * n_in + inner, rep * (depth // 4), 3 * depth // 4)
+        whole = p >= 3
+        base, size = (0, depth) if whole else (rep * (depth // 4), 3 * depth // 4)
+        ref = slot(p, src * n_in + inner, base, size)
         way = right.astype(jnp.int32)
         device = {"fs": (outer + 2 * way - 1) * n_in + inner}
         return moved(ref, z_send.at[p, way, src], z_recv.at[p, src], device)
 
+    def e_copy(p, src, right):
+        ref = slot(p, src * n_in + peer_in, 0, cut)
+        way = right.astype(jnp.int32)
+        device = {"fs": (outer + 2 * way - 1) * n_in + inner}
+        return moved(ref, e_send.at[p - 3, way, src], e_recv.at[p - 3, src], device)
+
     def y_copy(p, src):
-        ref = slot(p, src * n_in + inner, rep * (depth // 2), depth // 2)
+        base, size = (cut, depth - cut) if p >= 3 else (rep * (depth // 2), depth // 2)
+        ref = slot(p, src * n_in + inner, base, size)
         return moved(ref, y_send.at[p, src], y_recv.at[p, src], across)
 
     def y_own(p):
-        ref = slot(p, member, rep * (depth // 8), 7 * depth // 8)
+        base, size = (0, depth) if p >= 3 else (rep * (depth // 8), 7 * depth // 8)
+        ref = slot(p, member, base, size)
         return moved(ref, y_send.at[p, outer], y_recv.at[p, outer], across)
 
     def x_own(p):
@@ -96,13 +109,22 @@
     yes = outer >= 0
 
     def own_start(p):
-        pl.when(has_right)(lambda: z_copy(p, outer, yes).start())
-        pl.when(has_left)(lambda: z_copy(p, outer, outer < 0).start())
+        both_ways(z_copy, p, begin)
         y_own(p).start()
+
+    def both_ways(copy, p, act):
+        pl.when(has_right)(lambda: act(copy(p, outer, yes)))
+        pl.when(has_left)(lambda: act(copy(p, outer, outer < 0)))
+
+    def begin(copy):
+        copy.start()
 
     def own_finish(p):
         y_own(p).wait_recv()
-        x_own(p).start()
+        if p < 3:
+            x_own(p).start()
+        else:
+            both_ways(e_copy, p, begin)
 
     def onward(src):
         return jnp.where(src < outer, has_right, has_left)
@@ -112,52 +134,67 @@
         z_copy(p, src, src < outer).wait_recv()
         pl.when(onward(src))(lambda: z_copy(p, src, src < outer).start())
         y_copy(p, src).start()
-        x_side(p, src).start()
+        if p < 3:
+            x_side(p, src).start()
 
     def second_stage(p, k):
         src = source(k)
-        y_copy(p, src).wait_recv()
-        x_diag(p, src).start()
-
-    lag = 2
+        if p < 3:
+            y_copy(p, src).wait_recv()
+            x_diag(p, src).start()
+        else:
+            e_copy(p, src, src < outer).wait_recv()
+            pl.when(onward(src))(lambda: e_copy(p, src, src < outer).start())
+
     others = n_out - 1
 
     def comm(p, k):
         @pl.when(k == 0)
         def _():
-            pl.when(p + 2 < parts)(lambda: own_start(p + 2))
             own_finish(p)
+            if p > 0:
+                second_stage(p - 1, others)
 
         @pl.when(k > 0)
         def _():
             first_stage(p, k)
-            late = p * others + k - 1 - lag
-            pl.when(late >= 0)(lambda: second_stage(late // others, late % others + 1))
+            pl.when(k > 1)(lambda: second_stage(p, k - 1))
 
     def finish(p):
-        x_own(p).wait_recv()
+        if p < 3:
+            x_own(p).wait_recv()
 
         @pl.loop(1, n_out)
         def _(k):
             src = source(k)
-            x_side(p, src).wait_recv()
-            x_diag(p, src).wait_recv()
+            if p < 3:
+                x_side(p, src).wait_recv()
+                x_diag(p, src).wait_recv()
+            else:
+                y_copy(p, src).wait_recv()
+
+    def settle(copy):
+        copy.wait_send()
 
     def drain():
-        @pl.loop(0, parts)
-        def _(p):
-            pl.when(has_right)(lambda: z_copy(p, outer, yes).wait_send())
-            pl.when(has_left)(lambda: z_copy(p, outer, outer < 0).wait_send())
+        for p in range(parts):
+            both_ways(z_copy, p, settle)
             y_own(p).wait_send()
-            x_own(p).wait_send()
+            if p < 3:
+                x_own(p).wait_send()
+            else:
+                both_ways(e_copy, p, settle)
 
             @pl.loop(1, n_out)
             def _(k):
                 src = source(k)
                 pl.when(onward(src))(lambda: z_copy(p, src, src < outer).wait_send())
                 y_copy(p, src).wait_send()
-                x_side(p, src).wait_send()
-                x_diag(p, src).wait_send()
+                if p < 3:
+                    x_side(p, src).wait_send()
+                    x_diag(p, src).wait_send()
+                else:
+                    pl.when(onward(src))(lambda: e_copy(p, src, src < outer).wait_send())
 
     def tile(p):
         return pl.ds((p % n_out) * depth, depth), (p // n_out) * branch
@@ -166,18 +203,18 @@
         low, left = tile(p)
         if p < 2 or 3 <= p < 3 + n_ffn:
             src = (v_weight, u_weight)[p] if p < 2 else up_weight
-            first = 0 if p < 2 else (p - 3) * branch
+            first = 0 if p < 2 else rep * shared + (p - 3) * branch
             return [
                 pltpu.make_async_copy(
-                    src.at[:, pl.ds(first, branch)],
+                    src.at[:, pl.ds(first if p < 2 else pl.multiple_of(first, branch), branch)],
                     acc.at[low, pl.ds(left, branch)],
                     load_sem.at[p, 0],
                 )
             ]
-        src, first = (out_weight, 0) if p == 2 else (down_weight, (p - 3 - n_ffn) * branch)
+        src, first = (out_weight, outer * 0) if p == 2 else (down_weight, rep * shared + (p - 3 - n_ffn) * branch)
         return [
             pltpu.make_async_copy(
-                src.at[pl.ds(first + i * depth, depth), :],
+                src.at[pl.ds(pl.multiple_of(first + i * depth, depth), depth), :],
                 acc.at[low, pl.ds(left + i * depth, depth)],
                 load_sem.at[p, i],
             )
@@ -262,7 +299,7 @@
 
     def p_copy(k):
         r = here(k)
-        return remote(h_buf.at[r, :], p_recv.at[r, :], c_send.at[k, 0], c_recv.at[k, 0], mate)
+        return remote(terms.at[0, r, :], p_recv.at[r, :], c_send.at[k, 0], c_recv.at[k, 0], mate)
 
     def times(values, p, m):
         total = dot(values[:, :depth], gathered[p, m, :, pl.ds(0, depth)])
@@ -273,8 +310,6 @@
         return total
 
     def out_stage(k):
-        pl.when(k == 0)(lambda: stat_copy.wait())
-        pl.when(k > 0)(lambda: p_copy(k - 1).start())
         r = here(k)
         sums = own_stat[r, :] + mate_stat[0, r, :]
         centre = sums[:, 0:1] / (2 * branch)
@@ -299,13 +334,12 @@
         gate = jnp.concatenate(gates, axis=0)
         gated = (acc[r, pl.ds(branch, branch)] * gate).astype(half)
         for m in range(members):
-            h_buf[r, pl.ds(m * depth, depth)] = times(gated, 2, m).astype(half)
+            terms[0, r, pl.ds(m * depth, depth)] = times(gated, 2, m).astype(half)
 
     def mid_stage(k):
-        pl.when(k == 0)(lambda: p_copy(n_out - 1).start())
         p_copy(k).wait()
         r = here(k)
-        mix = h_buf[r, :].astype(single) + p_recv[r, :].astype(single)
+        mix = terms[0, r, :].astype(single) + p_recv[r, :].astype(single)
         scale = lax.rsqrt(jnp.sum(mix * mix, axis=1, keepdims=True) / width + 1e-06)
         mix = mix * scale * gain_mix_out[...]
         a = (stream[0, r, :].astype(single) + mix[:, :part]).astype(half)
@@ -318,120 +352,271 @@
         x_buf[r, pl.ds(0, part)] = (a * scale * gain_ffn_in[:, :part]).astype(half)
         x_buf[r, pl.ds(part, part)] = (b * scale * gain_ffn_in[:, part:]).astype(half)
 
-    def strip(j):
-        return pl.ds(pl.multiple_of(j * branch, branch), branch)
-
-    def up_stage(k, p):
-        r, cols = here(k), strip(p - 3)
-        raised = jax.nn.relu(dot(x_buf[r, :], spanned(p)) * up_scale[:, cols])
-        h_buf[r, cols] = (raised * raised).astype(half)
-
-    def down_stage(k, p, fresh):
-        r = here(k)
-        values = h_buf[r, strip(p - 3 - n_ffn)]
-        for m in range(members):
-            cols = pl.ds(m * depth, depth)
-            terms = times(values, p, m)
-            acc[r, cols] = terms if fresh else acc[r, cols] + terms
-
-    def segment(p, needs, *stages):
+    half_cols = pl.ds(pl.multiple_of(tp * part, part), part)
+
+    def a_copy(k):
+        r = here(k)
+        return remote(
+            x_buf.at[r, half_cols], x_twin.at[r, half_cols], a_send.at[k, 0], a_recv.at[k, 0], twin
+        )
+
+    def b_copy(k):
+        r = here(k)
+        return remote(
+            x_twin.at[r, half_cols], x_twin.at[r, half_cols], a_send.at[k, 1], a_recv.at[k, 1], mate
+        )
+
+    def pass_on(k):
+        a_copy(k).wait_recv()
+        b_copy(k).start()
+
+    def up_stage(w, k, j):
+        r = here(k)
+        source_rows = x_twin if w else x_buf
+        scale = up_scale[:, pl.ds(pl.multiple_of(rep * shared + j * branch, branch), branch)]
+        raised = jax.nn.relu(dot(source_rows[r, :], spanned(3 + j)) * scale)
+        h_buf[w, r, pl.ds(j * branch, branch)] = (raised * raised).astype(half)
+
+    planes = n_out // 2
+    block_cols = n_in * depth
+
+    def wide(src):
+        return pl.ds(pl.multiple_of(src * block_cols, block_cols), block_cols)
+
+    def narrow(src):
+        return wide(src % planes)
+
+    def d_copy(src, q):
+        w, r = (0, pl.ds(0, rows)) if q is None else (1, pl.ds(q * (rows // 2), rows // 2))
+        lane = 0 if q is None else 1 + q
+        return remote(
+            terms.at[w, r, wide(src)],
+            d_recv.at[w, r, narrow(src)],
+            d_send.at[lane, src],
+            d_sem.at[lane, src],
+            mate,
+        )
+
+    def o_copy(src, q):
+        r = pl.ds(q * (rows // 2), rows // 2)
+        return remote(
+            terms.at[1, r, wide(src)],
+            o_recv.at[r, narrow(src)],
+            o_send.at[src, q],
+            o_sem.at[src, q],
+            twin,
+        )
+
+    def mine(src):
+        return src // planes == tp
+
+    def down(k, q):
+        src = source(k)
+        w, low, high = (0, 0, n_out) if q is None else (1, q * planes, (q + 1) * planes)
+
+        @pl.loop(low, high)
+        def _(c):
+            r = here(c)
+            values = h_buf[w, r, :]
+            for i in range(n_in):
+                m = src * n_in + i
+                total = times(values[:, :branch], 3 + n_ffn, m)
+                for j in range(1, n_ffn):
+                    total += times(values[:, j * branch : (j + 1) * branch], 3 + n_ffn + j, m)
+                cols = pl.ds(pl.multiple_of(m * depth, depth), depth)
+                terms[w, r, cols] = total.astype(half)
+
+        pl.when(jnp.logical_not(mine(src)))(lambda: d_copy(src, q).start())
+
+    def merge(k, q):
+        src = source(k)
+
+        @pl.when(mine(src))
+        def _():
+            d_copy(src, q).wait_recv()
+
+            @pl.loop(q * planes, (q + 1) * planes)
+            def _(c):
+                r = here(c)
+                total = terms[1, r, wide(src)].astype(single)
+                total += d_recv[1, r, narrow(src)].astype(single)
+                terms[1, r, wide(src)] = total.astype(half)
+
+            o_copy(src, q).start()
+
+    def gather_group(k):
+        src = source(k)
+
+        @pl.when(mine(src))
+        def _():
+            d_copy(src, None).wait_recv()
+            o_copy(src, 0).wait_recv()
+            o_copy(src, 1).wait_recv()
+
+            @pl.loop(0, n_out)
+            def _(c):
+                r = here(c)
+                total = terms[0, r, wide(src)].astype(single)
+                total += d_recv[0, r, narrow(src)].astype(single)
+                total += o_recv[r, narrow(src)].astype(single)
+                acc[r, narrow(src)] = total
+                power = jnp.sum(total * total, axis=1, keepdims=True)
+                own_stat[r, :] += jnp.broadcast_to(power, (chunk, 128))
+
+    def segment(p, *stages):
         @pl.loop(0, n_out)
         def _(k):
             comm(p, k)
-            if needs is not None:
-                pl.when(k == 0)(lambda: finish(needs))
             for stage in stages:
                 stage(k)
 
-    segment(0, None)
-    segment(1, None, norm_stage)
-    segment(2, 0, v_stage)
-    segment(3, 1, u_stage)
-    segment(4, 2, out_stage)
-    segment(5, 3, mid_stage, lambda k: up_stage(k, 3))
-
-    @pl.loop(6, 5 + n_ffn)
-    def _(p):
-        segment(p, p - 2, lambda k: up_stage(k, p - 2))
-
-    for p in range(5 + n_ffn, parts):
-        segment(p, p - 2, lambda k: down_stage(k, p - 2, p == 5 + n_ffn))
-    last = parts - 1
-    for late in range(parts * others - lag, parts * others):
-        second_stage(late // others, late % others + 1)
-
-    finish(last - 1)
+    def each(stage):
+        pl.loop(0, n_out)(stage)
+
+    up_parts = range(3, 3 + n_ffn)
+    down_parts = range(3 + n_ffn, parts)
+    final = n_out - 1
+    middle = jnp.logical_and(has_left, has_right)
+
+    def nearest(stage, p):
+        stage(p, 1)
+        pl.when(middle)(lambda: stage(p, 2))
+
+    def second(stage, p):
+        stage(p, jnp.where(middle, 3, 2))
+
+    def third(stage, p):
+        pl.when(jnp.logical_not(middle))(lambda: stage(p, 3))
+
+    segment(0)
+    own_start(2)
+    segment(1, norm_stage)
+    finish(0)
+    segment(2, v_stage)
+    own_start(3)
+    own_start(4)
+    second_stage(2, others)
+    finish(1)
+    each(u_stage)
+    finish(2)
+    stat_copy.wait()
+    for k in range(n_out + 1):
+        if k < n_out:
+            out_stage(k)
+        if k > 0:
+            mid_stage(k - 1)
+        if k < n_out:
+            p_copy(k).start()
+        if k > 0:
+            a_copy(k - 1).start()
+        if 0 < k < n_out - 1:
+            nearest(first_stage, 2 + k)
+    own_stat[...] = jnp.zeros_like(own_stat)
+    own_finish(3)
+    own_finish(4)
+
+    def twin_up(k):
+        b_copy(k).wait_recv()
+        for j in range(n_ffn):
+            up_stage(1, k, j)
+
+    def arrive(k):
+        for p in down_parts:
+            y_copy(p, source(k)).wait_recv()
+
+    second(first_stage, 3)
+    nearest(second_stage, 3)
+    pass_on(0)
+    second(first_stage, 4)
+    own_start(5)
+    own_start(6)
+    nearest(second_stage, 4)
+    third(first_stage, 3)
+    second(second_stage, 3)
+    pass_on(1)
+    third(first_stage, 4)
+    second(second_stage, 4)
+    third(second_stage, 3)
+    third(second_stage, 4)
+    own_finish(5)
+    finish(3)
+    own_finish(6)
+    finish(4)
+    twin_up(0)
+    twin_up(1)
+    down(0, 0)
+    for p in down_parts:
+        nearest(first_stage, p)
+    pass_on(2)
+    each(lambda k: up_stage(0, k, 0))
+    merge(0, 0)
+    for p in down_parts:
+        nearest(second_stage, p)
+    arrive(1)
+    down(1, 0)
+    twin_up(2)
+    merge(1, 0)
+    each(lambda k: up_stage(0, k, 1))
+    pass_on(3)
+    for p in down_parts:
+        second(first_stage, p)
+    twin_up(3)
+    down(0, 1)
+    down(1, 1)
+    merge(0, 1)
+    for p in down_parts:
+        second(second_stage, p)
+    merge(1, 1)
+    down(0, None)
+    down(1, None)
+    arrive(2)
+    down(2, 0)
+    down(2, 1)
+    for p in down_parts:
+        third(first_stage, p)
+    merge(2, 0)
+    merge(2, 1)
+    for p in down_parts:
+        third(second_stage, p)
+    down(2, None)
+    arrive(3)
+    down(3, 0)
+    down(3, 1)
+    merge(3, 0)
+    merge(3, 1)
+    down(3, None)
+    each(gather_group)
+    s_copy = remote(own_stat, mate_stat.at[1], c_send.at[0, 1], c_recv.at[0, 1], mate)
+    s_copy.start()
+    drain()
+    for k in range(n_out):
+        a_copy(k).wait_send()
+        b_copy(k).wait_send()
+
+        @pl.when(mine(k))
+        def _():
+            o_copy(k, 0).wait_send()
+            o_copy(k, 1).wait_send()
+
+        @pl.when(jnp.logical_not(mine(k)))
+        def _():
+            d_copy(k, None).wait_send()
+            d_copy(k, 0).wait_send()
+            d_copy(k, 1).wait_send()
+
+    s_copy.wait()
+
+    def leave(k):
+        r = here(k)
+        return pltpu.make_async_copy(x_buf.at[r, pl.ds(0, part)], result.at[r, :], out_sem.at[k])
 
     @pl.loop(0, n_out)
     def _(k):
-        down_stage(k, last - 1, False)
-
-    finish(last)
-    share = members // 2
-
-    def f_copy(k):
-        r = here(k)
-        return remote(
-            x_buf.at[r, pl.ds(0, part)], f_recv.at[r, :], c_send.at[k, 1], c_recv.at[k, 1], mate
-        )
-
-    def s_copy(k):
-        r = here(k)
-        return remote(
-            own_stat.at[r, :], mate_stat.at[1, r, :], c_send.at[k, 0], c_recv.at[k, 0], mate
-        )
-
-    def own_cols(m):
-        return pl.ds(pl.multiple_of(m * depth, depth), depth)
-
-    @pl.loop(0, n_out)
-    def _(k):
-        r = here(k)
-        values = h_buf[r, pl.ds((n_ffn - 1) * branch, branch)]
-        for i in range(share):
-            m = (1 - tp) * share + i
-            terms = acc[r, own_cols(m)] + times(values, last, m)
-            x_buf[r, pl.ds(i * depth, depth)] = terms.astype(half)
-        pl.when(k > 0)(lambda: f_copy(k - 1).start())
-
-    f_copy(n_out - 1).start()
-
-    @pl.loop(0, n_out)
-    def _(k):
-        r = here(k)
-        values = h_buf[r, pl.ds((n_ffn - 1) * branch, branch)]
-        kept = []
-        for i in range(share):
-            m = tp * share + i
-            terms = acc[r, own_cols(m)] + times(values, last, m)
-            kept.append(terms.astype(half).astype(single))
-        f_copy(k).wait()
-        power = jnp.zeros((chunk, 1), single)
-        for i in range(share):
-            total = kept[i] + f_recv[r, pl.ds(i * depth, depth)].astype(single)
-            power += jnp.sum(total * total, axis=1, keepdims=True)
-            acc[r, own_cols(tp * share + i)] = total
-        own_stat[r, :] = jnp.broadcast_to(power, (chunk, 128))
-        pl.when(k > 0)(lambda: s_copy(k - 1).start())
-
-    s_copy(n_out - 1).start()
-    drain()
-
-    def leave(k):
-        r = here(k)
-        return pltpu.make_async_copy(
-            x_buf.at[r, pl.ds(part, part)], result.at[r, :], out_sem.at[k]
-        )
-
-    @pl.loop(0, n_out)
-    def _(k):
-        s_copy(k).wait()
         r = here(k)
         power = own_stat[r, 0:1] + mate_stat[1, r, 0:1]
         scale = lax.rsqrt(power / width + 1e-06)
-        cols = pl.ds(pl.multiple_of(tp * part, part), part)
-        total = acc[r, cols] * scale * gain_ffn_out[:, cols]
-        x_buf[r, pl.ds(part, part)] = (stream[tp, r, :].astype(single) + total).astype(half)
+        total = acc[r, :] * scale * gain_ffn_out[:, half_cols]
+        x_buf[r, pl.ds(0, part)] = (stream[tp, r, :].astype(single) + total).astype(half)
         leave(k).start()
 
     for k in range(n_out):
@@ -569,8 +754,8 @@
     members = lax.axis_size("fs")
     width = part * 2
     depth, branch = v_weight.shape
-    hidden = up_weight.shape[1]
-    parts = 3 + 2 * (hidden // branch)
+    shared = up_weight.shape[1] // 2
+    parts = 3 + 2 * (shared // branch)
     n_in = 2
     n_out = members // n_in
     half, single = jnp.bfloat16, jnp.float32
@@ -597,11 +782,14 @@
     dma = pltpu.SemaphoreType.DMA
     scratch = [
         pltpu.VMEM((parts, members, depth, branch), half),
-        pltpu.VMEM((rows, width), single),
+        pltpu.VMEM((rows, part), single),
+        pltpu.VMEM((rows, width), half),
         pltpu.VMEM((rows, width), half),
         pltpu.VMEM((2, rows, part), half),
+        pltpu.VMEM((2, rows, shared), half),
+        pltpu.VMEM((2, rows, width), half),
         pltpu.VMEM((rows, width), half),
-        pltpu.VMEM((rows, width), half),
+        pltpu.VMEM((2, rows, part), half),
         pltpu.VMEM((rows, part), half),
         pltpu.VMEM((rows, 128), single),
         pltpu.VMEM((2, rows, 128), single),
@@ -609,13 +797,21 @@
         pltpu.VMEM((block, branch), single),
         dma((parts, 2, n_out)),
         dma((parts, n_out)),
+        dma((parts - 3, 2, n_out)),
+        dma((parts - 3, n_out)),
         dma((parts, n_out)),
         dma((parts, n_out)),
-        dma((parts, n_out, 2)),
-        dma((parts, n_out, 2)),
+        dma((3, n_out, 2)),
+        dma((3, n_out, 2)),
         dma((parts, branch // depth)),
         dma((2,)),
         dma((2,)),
+        dma((n_out, 2)),
+        dma((n_out, 2)),
+        dma((n_out, 2)),
+        dma((n_out, 2)),
+        dma((3, n_out)),
+        dma((3, n_out)),
         dma((n_out, 2)),
         dma((n_out, 2)),
         dma((n_out,)),
@@ -666,10 +862,10 @@
         groups, block = args[7].shape[0] // sizes["tp"], args[7].shape[1]
         planes, depth = sizes["fs"] // 2, width // sizes["fs"]
         paired = sizes["rep"] == 2 and sizes["tp"] == 2 and sizes["fs"] % 4 == 0
-        fits = depth % 256 == 0 and branch % depth == 0 and hidden % branch == 0
+        fits = depth % 256 == 0 and branch % depth == 0 and hidden == 4 * branch
         blocks = rows % (planes * block) == 0 and (256 * groups) % branch == 0
         small = 2 * width * (3 * branch + 2 * hidden) <= 24 * 1024 * 1024
-        fast = paired and planes >= 2 and fits and blocks and small
+        fast = paired and planes == 4 and fits and blocks and small
         return mapped(local_fast if fast else local)(*args)
 
     def mapped(body):

time: 189 us -> 179 us (0.947)
  Pallas kernels: 186 us -> 176 us
    pallas_call x1, Pallas kernels: 186 us -> 176 us  [local_fast(): pl.pallas_call(functools.partial(fused_kernel, n_out, n_in), out_shape=ja...]
where the time goes in v2:
time: 179 us
  Pallas kernels  176 us (98%)
  local copies, waits for them, and re-layouts  3.08 us (2%)
    pallas_call x1, Pallas kernels, local_fast(): pl.pallas_call(functools.partial(fused_kernel, n_out, n_in), out_shape=ja...  176 us

profile of v2, /device:TPU:0, one launch (start us, length us, event | category | flops | bytes accessed | tf_op | source)
XLA Modules:
  0.0 178.7 jit_solution(11610221221299484597)
XLA Ops:
  0.0 175.6 %fused_layer.1 = bf16[1024,1024]{1,0:T(8,128)(2,1)} custom-call(bf16[1024,1024]{1,0:T(8,128)(2,1)} %refs_0_.1, f32[256,512]{1,0:T(8,128)} %refs_1_.1, f32[256,512]{1,0:T(8,128)} %refs_2_.1, f32[512,256]{1,0:T(8,128)} %refs_3_.1, f32[256,2048]{1,0:T(8,128)} %refs_4_.1, f32[2048,256]{1,0:T(8,128)} %refs_5_.1, f32[1,2048]{1,0:T(1,128)} %bitcast.10, ...), custom_call_target="tpu_custom_call" | custom-call | tf_op jit(solution)/shard_map/fused_layer/pallas_call | solution.py:819
  175.6 3.1 %copy.20 = bf16[1024,1024]{1,0:T(8,128)(2,1)} copy(bf16[1024,1024]{1,0:T(8,128)(2,1)} %fused_layer.1) | data formatting | bytes 4194304

commit v3 on v2

--- a/solution.py
+++ b/solution.py
@@ -386,8 +386,15 @@
     def narrow(src):
         return wide(src % planes)
 
+    early = n_out - 1
+    limits = ((0, early), (early, n_out))
+
+    def span_of(q):
+        low, high = limits[q]
+        return pl.ds(low * chunk, (high - low) * chunk)
+
     def d_copy(src, q):
-        w, r = (0, pl.ds(0, rows)) if q is None else (1, pl.ds(q * (rows // 2), rows // 2))
+        w, r = (0, pl.ds(0, rows)) if q is None else (1, span_of(q))
         lane = 0 if q is None else 1 + q
         return remote(
             terms.at[w, r, wide(src)],
@@ -398,7 +405,7 @@
         )
 
     def o_copy(src, q):
-        r = pl.ds(q * (rows // 2), rows // 2)
+        r = span_of(q)
         return remote(
             terms.at[1, r, wide(src)],
             o_recv.at[r, narrow(src)],
@@ -412,7 +419,7 @@
 
     def down(k, q):
         src = source(k)
-        w, low, high = (0, 0, n_out) if q is None else (1, q * planes, (q + 1) * planes)
+        w, low, high = (0, 0, n_out) if q is None else (1, *limits[q])
 
         @pl.loop(low, high)
         def _(c):
@@ -435,7 +442,7 @@
         def _():
             d_copy(src, q).wait_recv()
 
-            @pl.loop(q * planes, (q + 1) * planes)
+            @pl.loop(*limits[q])
             def _(c):
                 r = here(c)
                 total = terms[1, r, wide(src)].astype(single)
@@ -511,9 +518,8 @@
             a_copy(k - 1).start()
         if 0 < k < n_out - 1:
             nearest(first_stage, 2 + k)
+            own_finish(2 + k)
     own_stat[...] = jnp.zeros_like(own_stat)
-    own_finish(3)
-    own_finish(4)
 
     def twin_up(k):
         b_copy(k).wait_recv()
@@ -524,60 +530,62 @@
         for p in down_parts:
             y_copy(p, source(k)).wait_recv()
 
+    nearest(second_stage, 3)
     second(first_stage, 3)
-    nearest(second_stage, 3)
     pass_on(0)
+    nearest(second_stage, 4)
     second(first_stage, 4)
-    own_start(5)
-    own_start(6)
-    nearest(second_stage, 4)
+    second(second_stage, 3)
     third(first_stage, 3)
-    second(second_stage, 3)
+    second(second_stage, 4)
+    both_ways(z_copy, 5, begin)
+    both_ways(z_copy, 6, begin)
     pass_on(1)
     third(first_stage, 4)
-    second(second_stage, 4)
+    y_own(5).start()
+    y_own(6).start()
     third(second_stage, 3)
     third(second_stage, 4)
-    own_finish(5)
     finish(3)
-    own_finish(6)
     finish(4)
     twin_up(0)
     twin_up(1)
+    own_finish(5)
+    pass_on(2)
+    nearest(first_stage, 5)
+    each(lambda k: up_stage(0, k, 0))
+    twin_up(2)
+    own_finish(6)
     down(0, 0)
-    for p in down_parts:
-        nearest(first_stage, p)
-    pass_on(2)
-    each(lambda k: up_stage(0, k, 0))
+    nearest(first_stage, 6)
     merge(0, 0)
-    for p in down_parts:
-        nearest(second_stage, p)
+    each(lambda k: up_stage(0, k, 1))
+    pass_on(3)
+    nearest(second_stage, 5)
+    nearest(second_stage, 6)
+    twin_up(3)
+    down(0, 1)
     arrive(1)
     down(1, 0)
-    twin_up(2)
+    merge(0, 1)
+    second(first_stage, 5)
+    down(1, 1)
     merge(1, 0)
-    each(lambda k: up_stage(0, k, 1))
-    pass_on(3)
-    for p in down_parts:
-        second(first_stage, p)
-    twin_up(3)
-    down(0, 1)
-    down(1, 1)
-    merge(0, 1)
-    for p in down_parts:
-        second(second_stage, p)
     merge(1, 1)
+    second(first_stage, 6)
     down(0, None)
-    down(1, None)
+    second(second_stage, 5)
+    second(second_stage, 6)
+    third(first_stage, 5)
     arrive(2)
     down(2, 0)
     down(2, 1)
-    for p in down_parts:
-        third(first_stage, p)
     merge(2, 0)
     merge(2, 1)
-    for p in down_parts:
-        third(second_stage, p)
+    third(first_stage, 6)
+    down(1, None)
+    third(second_stage, 5)
+    third(second_stage, 6)
     down(2, None)
     arrive(3)
     down(3, 0)

time: 179 us -> 169 us (0.944)
  Pallas kernels: 176 us -> 166 us
    pallas_call x1, Pallas kernels: 176 us -> 166 us  [local_fast(): pl.pallas_call(functools.partial(fused_kernel, n_out, n_in), out_shape=ja...]
where the time goes in v3:
time: 169 us
  Pallas kernels  166 us (98%)
  local copies, waits for them, and re-layouts  3.08 us (2%)
    pallas_call x1, Pallas kernels, local_fast(): pl.pallas_call(functools.partial(fused_kernel, n_out, n_in), out_shape=ja...  166 us

profile of v3, /device:TPU:0, one launch (start us, length us, event | category | flops | bytes accessed | tf_op | source)
XLA Modules:
  0.0 169.1 jit_solution(13743452099045486822)
XLA Ops:
  0.0 166.1 %fused_layer.1 = bf16[1024,1024]{1,0:T(8,128)(2,1)} custom-call(bf16[1024,1024]{1,0:T(8,128)(2,1)} %refs_0_.1, f32[256,512]{1,0:T(8,128)} %refs_1_.1, f32[256,512]{1,0:T(8,128)} %refs_2_.1, f32[512,256]{1,0:T(8,128)} %refs_3_.1, f32[256,2048]{1,0:T(8,128)} %refs_4_.1, f32[2048,256]{1,0:T(8,128)} %refs_5_.1, f32[1,2048]{1,0:T(1,128)} %bitcast.10, ...), custom_call_target="tpu_custom_call" | custom-call | tf_op jit(solution)/shard_map/fused_layer/pallas_call | solution.py:827
  166.1 3.1 %copy.20 = bf16[1024,1024]{1,0:T(8,128)(2,1)} copy(bf16[1024,1024]{1,0:T(8,128)(2,1)} %fused_layer.1) | data formatting | bytes 4194304

commit v4 on v3

--- a/solution.py
+++ b/solution.py
@@ -451,16 +451,16 @@
 
             o_copy(src, q).start()
 
-    def gather_group(k):
+    def gather_group(k, q):
         src = source(k)
 
         @pl.when(mine(src))
         def _():
-            d_copy(src, None).wait_recv()
-            o_copy(src, 0).wait_recv()
-            o_copy(src, 1).wait_recv()
-
-            @pl.loop(0, n_out)
+            if q == 0:
+                d_copy(src, None).wait_recv()
+            o_copy(src, q).wait_recv()
+
+            @pl.loop(*limits[q])
             def _(c):
                 r = here(c)
                 total = terms[0, r, wide(src)].astype(single)
@@ -593,13 +593,37 @@
     merge(3, 0)
     merge(3, 1)
     down(3, None)
-    each(gather_group)
-    s_copy = remote(own_stat, mate_stat.at[1], c_send.at[0, 1], c_recv.at[0, 1], mate)
-    s_copy.start()
     drain()
+
+    def s_copy(q):
+        r = span_of(q)
+        return remote(
+            own_stat.at[r, :], mate_stat.at[1, r, :], c_send.at[q, 1], c_recv.at[q, 1], mate
+        )
+
+    def leave(k):
+        r = here(k)
+        return pltpu.make_async_copy(x_buf.at[r, pl.ds(0, part)], result.at[r, :], out_sem.at[k])
+
     for k in range(n_out):
         a_copy(k).wait_send()
         b_copy(k).wait_send()
+
+    for q in range(2):
+        each(lambda k: gather_group(k, q))
+        s_copy(q).start()
+        s_copy(q).wait()
+
+        @pl.loop(*limits[q])
+        def _(k):
+            r = here(k)
+            power = own_stat[r, 0:1] + mate_stat[1, r, 0:1]
+            scale = lax.rsqrt(power / width + 1e-06)
+            total = acc[r, :] * scale * gain_ffn_out[:, half_cols]
+            x_buf[r, pl.ds(0, part)] = (stream[tp, r, :].astype(single) + total).astype(half)
+            leave(k).start()
+
+    for k in range(n_out):
 
         @pl.when(mine(k))
         def _():
@@ -611,21 +635,6 @@
             d_copy(k, None).wait_send()
             d_copy(k, 0).wait_send()
             d_copy(k, 1).wait_send()
-
-    s_copy.wait()
-
-    def leave(k):
-        r = here(k)
-        return pltpu.make_async_copy(x_buf.at[r, pl.ds(0, part)], result.at[r, :], out_sem.at[k])
-
-    @pl.loop(0, n_out)
-    def _(k):
-        r = here(k)
-        power = own_stat[r, 0:1] + mate_stat[1, r, 0:1]
-        scale = lax.rsqrt(power / width + 1e-06)
-        total = acc[r, :] * scale * gain_ffn_out[:, half_cols]
-        x_buf[r, pl.ds(0, part)] = (stream[tp, r, :].astype(single) + total).astype(half)
-        leave(k).start()
 
     for k in range(n_out):
         leave(k).wait()

time: 169 us -> 168 us (level)
  Pallas kernels: 166 us -> 164 us
    pallas_call x1, Pallas kernels: 166 us -> 164 us  [local_fast(): pl.pallas_call(functools.partial(fused_kernel, n_out, n_in), out_shape=ja...]
where the time goes in v4:
time: 168 us; the launch traced here: 167 us
  Pallas kernels  164 us (98%)
  local copies, waits for them, and re-layouts  3.08 us (2%)
    pallas_call x1, Pallas kernels, local_fast(): pl.pallas_call(functools.partial(fused_kernel, n_out, n_in), out_shape=ja...  164 us

profile of v4, /device:TPU:0, one launch (start us, length us, event | category | flops | bytes accessed | tf_op | source)
XLA Modules:
  0.0 167.4 jit_solution(15517795381289090051)
XLA Ops:
  0.0 164.3 %fused_layer.1 = bf16[1024,1024]{1,0:T(8,128)(2,1)} custom-call(bf16[1024,1024]{1,0:T(8,128)(2,1)} %refs_0_.1, f32[256,512]{1,0:T(8,128)} %refs_1_.1, f32[256,512]{1,0:T(8,128)} %refs_2_.1, f32[512,256]{1,0:T(8,128)} %refs_3_.1, f32[256,2048]{1,0:T(8,128)} %refs_4_.1, f32[2048,256]{1,0:T(8,128)} %refs_5_.1, f32[1,2048]{1,0:T(1,128)} %bitcast.10, ...), custom_call_target="tpu_custom_call" | custom-call | tf_op jit(solution)/shard_map/fused_layer/pallas_call | solution.py:836
  164.3 3.1 %copy.20 = bf16[1024,1024]{1,0:T(8,128)(2,1)} copy(bf16[1024,1024]{1,0:T(8,128)(2,1)} %fused_layer.1) | data formatting | bytes 4194304
